TPU v7x, 32 devices: a whole 2x2x4 slice. The times are simulated.
32 devices in a mesh: grp: 2 (over y), sp: 4 (over z), dp: 4 (over x, core).
Axes of the slice: x: 2, y: 2, z: 4, core: 2. Of those that a mesh axis runs over, the one named last changes fastest.
Arguments:
- mixer_source_array: bfloat16 [8, 768, 2048], P(('grp', 'dp'), 'sp'), parts along dimension 0, may hold values from -6 to 6
- source_projection: bfloat16 [2048, 1024], P('dp'), may hold values from -0.125 to 0.125
- gating_projection: bfloat16 [2048, 1024], P('dp'), may hold values from -0.125 to 0.125
- entry_mapping_projection: bfloat16 [2048, 256], replicated, may hold values from -0.0390625 to 0.0390625
- readout_mapping_projection: bfloat16 [2048, 256], replicated, may hold values from -0.0390625 to 0.0390625
- increment_projection: bfloat16 [2048, 16], replicated, may hold values from -0.125 to 0.125
- source_conv_taps: float32 [4, 1024], replicated, may hold values from -3 to 3
- entry_mapping_taps: float32 [4, 256], replicated, may hold values from -3 to 3
- readout_mapping_taps: float32 [4, 256], replicated, may hold values from -3 to 3
- increment_offsets: float32 [16], replicated, may hold values from -1 to 1
- channel_damping_rate: float32 [16], replicated, may hold values from 0 to 1
- bypass_coefficients: float32 [16], replicated, may hold values from 0.5 to 1.5
- stride_multiplier: float32 [8, 768], P(('grp', 'dp')), parts along dimension 0, may hold values from 0.5 to 2
- added_log_damping: float32 [8, 768, 16], P(('grp', 'dp')), parts along dimension 0, may hold values from -2.1 to 0
- norm_scale_factor: float32 [1024], replicated, may hold values from 0.1 to 1.9
- final_projection: bfloat16 [1024, 2048], P(None, 'dp'), may hold values from -0.1875 to 0.1875
Outputs:
- output: bfloat16 [8, 768, 2048], P(('grp', 'dp'), 'sp'), parts along dimension 0
There are 2 independent parts, one for each index of `grp`. A program takes and returns all parts, laid end to end along the dimension named above; an argument that names none is the same for every part. Nothing has to cross between parts.
All inputs are finite; a program needn't handle non-finite values.
Results may differ from a plain program's by a relative error of at most 0.015.
Values may be sent and summed in bfloat16 or wider, within the bound.
A program may use at most 64 MiB of HBM per device.

v0:
```python
import functools

import jax
import jax.numpy as jnp
from jax import lax
from jax.experimental import pallas as pl
from jax.experimental.pallas import tpu as pltpu
from jax.sharding import PartitionSpec as P

P_SIZE = 64
N = 128
G = 2
CONV_W = 4
EPSILON = 1e-06
HIGH = lax.Precision.HIGHEST
MESH = pl.DeviceIdType.MESH
HALO = 16
F32 = jnp.float32
BF16 = jnp.bfloat16


def dot(a, b, dims=((1,), (0,)), precision=None):
    return lax.dot_general(a, b, (dims, ((), ())), precision=precision, preferred_element_type=F32)


def silu(v):
    return v * (1.0 / (1.0 + jnp.exp(-v)))


def kernel(
    dims,
    x_hbm,
    wx_hbm,
    wz_hbm,
    wf_hbm,
    wb_hbm,
    wc_hbm,
    wdt_hbm,
    tx_ref,
    tb_ref,
    tc_ref,
    off_ref,
    rate_ref,
    skip_ref,
    stride_ref,
    damp_ref,
    scale_ref,
    out_hbm,
    xe,
    wx,
    wz,
    wf,
    pbc,
    px,
    bm,
    cm,
    xs,
    sc,
    y,
    st,
    car,
    snd,
    nrm,
    out_ref,
    wbc,
    wdt,
    loc_sem,
    halo_send,
    halo_recv,
    x_send,
    x_recv,
    y_send,
    y_recv,
    z_send,
    z_recv,
    d_send,
    d_recv,
    c_send,
    c_recv,
    o_sem,
):
    n_grp, n_sp, n_dp, c_chunks = dims
    n_x = n_dp // 2
    grp, z, dp = (lax.axis_index(a) for a in ("grp", "sp", "dp"))
    xi, core = dp // 2, dp % 2
    tok = out_ref.shape[0]
    width = xs.shape[1]
    heads = off_ref.shape[1]
    per_group = heads // G
    gw = width // G
    partner = {"dp": xi * 2 + 1 - core}
    y_peer = {"grp": 1 - grp}
    zb = z % 2
    z_peer = {"sp": z + 1 - 2 * zb}
    srcs = (wx_hbm, wz_hbm, wf_hbm)

    def at(w, owner, start, rows):
        if w == 2:
            return wf.at[owner, pl.ds(start, rows)]
        ref = (wx, wz)[w]
        return ref.at[pl.ds(pl.multiple_of(owner * srcs[w].shape[0] + start, 16), rows)]

    barrier = pltpu.get_barrier_semaphore()
    peers = [partner, y_peer]
    peers += [{"dp": lax.rem(xi + o, n_x) * 2 + core} for o in range(1, n_x)]
    for peer in peers:
        pl.semaphore_signal(barrier, inc=1, device_id=peer, device_id_type=MESH)

    @pl.when(z > 0)
    def _():
        pl.semaphore_signal(barrier, inc=1, device_id={"sp": z - 1}, device_id_type=MESH)

    @pl.when(z < n_sp - 1)
    def _():
        pl.semaphore_signal(barrier, inc=1, device_id={"sp": z + 1}, device_id_type=MESH)

    gn = G * N
    x_copy = pltpu.make_async_copy(x_hbm, xe.at[pl.ds(HALO, tok)], loc_sem.at[3])
    x_copy.start()
    maps = [
        pltpu.make_async_copy(wb_hbm, wbc.at[:, pl.ds(0, gn)], loc_sem.at[4]),
        pltpu.make_async_copy(wc_hbm, wbc.at[:, pl.ds(gn, gn)], loc_sem.at[5]),
        pltpu.make_async_copy(wdt_hbm, wdt, loc_sem.at[6]),
    ]
    for copy in maps:
        copy.start()
    own = []
    for w in range(3):
        copy = pltpu.make_async_copy(srcs[w], at(w, dp, 0, srcs[w].shape[0]), loc_sem.at[w])
        copy.start()
        own.append(copy)

    pl.semaphore_wait(barrier, len(peers) + jnp.minimum(z, 1) + jnp.minimum(n_sp - 1 - z, 1))

    def remote(src, dst, send, recv, peer):
        return pltpu.make_async_remote_copy(
            src_ref=src, dst_ref=dst, send_sem=send, recv_sem=recv,
            device_id=peer, device_id_type=MESH,
        )

    def halo_copy():
        return remote(
            x_hbm.at[pl.ds(tok - HALO, HALO)], xe.at[pl.ds(0, HALO)],
            halo_send, halo_recv, {"sp": jnp.minimum(z + 1, n_sp - 1)},
        )

    @pl.when(z < n_sp - 1)
    def _():
        halo_copy().start()

    sends = []

    def half_of(w):
        return srcs[w].shape[0] // 8

    def owner_of(o):
        return lax.rem(xi - o + n_x, n_x) * 2 + core

    own_q = grp * 2 + zb
    y_q = (1 - grp) * 2 + zb
    z_q = grp * 2 + 1 - zb
    far_q = (1 - grp) * 2 + 1 - zb

    def x_piece(w, o, k, owner, src=None):
        rows = half_of(w)
        start = far_q * 2 * rows + rows if k == 2 else own_q * 2 * rows + k * rows
        place = at(w, owner, start, rows)
        if src is not None:
            src = src.at[pl.ds(pl.multiple_of(start, 16), rows)]
        return remote(
            place if src is None else src, place,
            x_send.at[w, o - 1, k], x_recv.at[w, o - 1, k],
            {"dp": lax.rem(xi + o, n_x) * 2 + core},
        )

    def y_piece(w, o, k, quarter, part):
        place = at(w, owner_of(o), (quarter * 2 + part) * half_of(w), half_of(w))
        return remote(place, place, y_send.at[w, o - 1, k], y_recv.at[w, o - 1, k], y_peer)

    def z_piece(w, o, k, quarter):
        place = at(w, owner_of(o), (quarter * 2 + k) * half_of(w), half_of(w))
        return remote(place, place, z_send.at[w, o - 1, k], z_recv.at[w, o - 1, k], z_peer)

    def d_piece(w, o, k, quarter):
        place = at(w, owner_of(o), quarter * 2 * half_of(w), 2 * half_of(w))
        return remote(place, place, d_send.at[w, o, k], d_recv.at[w, 1], partner)

    def start(copy):
        copy.start()
        sends.append(copy)

    for w in range(3):
        for k in range(3):
            for o in range(1, n_x):
                start(x_piece(w, o, k, dp, srcs[w]))
        rows = srcs[w].shape[0]
        start(remote(srcs[w], at(w, dp, 0, rows), d_send.at[w, 0, 0], d_recv.at[w, 0], partner))

    def pump(w, k):
        for o in range(1, n_x):
            if k < 2:
                x_piece(w, o, k, owner_of(o)).wait_recv()
                start(y_piece(w, o, k, own_q, k))
                start(z_piece(w, o, k, own_q))
                if k == 1:
                    start(d_piece(w, o, 0, own_q))
            elif k == 2:
                z_piece(w, o, 0, z_q).wait_recv()
                start(y_piece(w, o, 2, z_q, 0))
            elif k == 3:
                z_piece(w, o, 1, z_q).wait_recv()
                start(d_piece(w, o, 1, z_q))
                y_piece(w, o, 0, y_q, 0).wait_recv()
                y_piece(w, o, 1, y_q, 1).wait_recv()
                start(d_piece(w, o, 2, y_q))
            else:
                y_piece(w, o, 2, far_q, 0).wait_recv()
                x_piece(w, o, 2, owner_of(o)).wait_recv()
                start(d_piece(w, o, 3, far_q))

    def finish_near(w):
        own[w].wait()
        place = at(w, dp, 0, srcs[w].shape[0])
        remote(place, place, d_send.at[w, 0, 0], d_recv.at[w, 0], partner).wait_recv()

    def finish_far(w):
        if w == 2:
            place = wf.at[pl.ds(0, n_x - 1)]
        else:
            place = (wx, wz)[w].at[pl.ds(0, (n_x - 1) * srcs[w].shape[0])]
        remote(place, place, d_send.at[w, 1, 0], d_recv.at[w, 1], partner).wait_recv()

    depth = 2 * wx_hbm.shape[0]

    def chip_rows(o):
        return pl.ds(pl.multiple_of(lax.rem(xi - o + n_x, n_x) * depth, 128), depth)

    @pl.when(z == 0)
    def _():
        xe[pl.ds(0, HALO), :] = jnp.zeros((HALO, xe.shape[1]), BF16)

    @pl.when(z > 0)
    def _():
        halo_copy().wait_recv()

    x_copy.wait()
    for copy in maps:
        copy.wait()
    pbc[...] = dot(xe[...], wbc[...]).astype(BF16).astype(F32)
    raw = dot(wdt[...], xe[pl.ds(HALO, tok), :], ((1,), (1,))).astype(BF16).astype(F32)

    def conv(buf, cols, taps):
        total = taps[0:1, :] * buf[pl.ds(HALO - CONV_W + 1, tok), cols]
        for k in range(1, CONV_W):
            total = total + taps[k : k + 1, :] * buf[pl.ds(HALO - CONV_W + 1 + k, tok), cols]
        return silu(total).astype(BF16)

    bm[...] = conv(pbc, pl.ds(0, gn), tb_ref[...])
    cm[...] = conv(pbc, pl.ds(gn, gn), tc_ref[...])

    def square_iota(size):
        return [lax.broadcasted_iota(jnp.int32, (size, size), d) for d in (0, 1)]

    def column(ref):
        i, j = square_iota(heads)
        return jnp.sum(jnp.where(i == j, ref[...], 0.0), axis=1, keepdims=True)

    def my_positions(values):
        mine = values[:, 0:tok]
        for i in range(1, n_sp):
            mine = jnp.where(z == i, values[:, i * tok : (i + 1) * tok], mine)
        return mine

    pre = raw + column(off_ref)
    step_t = jnp.maximum(pre, 0.0) + jnp.log1p(jnp.exp(-jnp.abs(pre)))
    tempo = my_positions(stride_ref[...])
    keep = -column(rate_ref) * step_t * tempo + my_positions(damp_ref[0])
    row, col = square_iota(tok)
    lower = row >= col
    step = dot((row == col).astype(F32), step_t, ((1,), (1,)), HIGH)
    cum = dot(lower.astype(F32), keep, ((1,), (1,)), HIGH)
    cum_t = dot(keep, (row <= col).astype(F32), precision=HIGH)
    last = cum[tok - 1 : tok, :]
    to_end = jnp.exp(last - cum)
    reach = jnp.exp(cum)
    whole = jnp.exp(last)
    first_head = lax.broadcasted_iota(jnp.int32, (tok, 2 * P_SIZE), 1) < P_SIZE
    first_row = first_head[0:1, :]

    def spread(values, p, mask):
        return jnp.where(mask, values[:, 2 * p : 2 * p + 1], values[:, 2 * p + 1 : 2 * p + 2])

    def pair_cols(p):
        return pl.ds(p * 2 * P_SIZE, 2 * P_SIZE)

    tile = 256

    def tiles(body):
        def run(j, carry):
            body(pl.ds(pl.multiple_of(j * tile, tile), tile))
            return carry

        lax.fori_loop(0, width // tile, run, 0)

    def near_x(cols):
        px[:, cols] = dot(xe[:, chip_rows(0)], wx[chip_rows(0), cols])

    def far_x(cols):
        acc = px[:, cols]
        for o in range(1, n_x):
            acc = acc + dot(xe[:, chip_rows(o)], wx[chip_rows(o), cols])
        px[:, cols] = acc.astype(BF16).astype(F32)
        xs[:, cols] = conv(px, cols, tx_ref[:, cols])

    rows = pl.ds(HALO, tok)

    def near_z(cols):
        px[pl.ds(0, tok), cols] = dot(xe[rows, chip_rows(0)], wz[chip_rows(0), cols])

    def far_z(cols):
        acc = px[pl.ds(0, tok), cols]
        for o in range(1, n_x):
            acc = acc + dot(xe[rows, chip_rows(o)], wz[chip_rows(o), cols])
        px[pl.ds(0, tok), cols] = silu(acc.astype(BF16).astype(F32))

    pump(0, 0)
    pump(0, 1)
    finish_near(0)
    tiles(near_x)
    pump(0, 2)
    pump(0, 3)
    pump(1, 0)
    pump(0, 4)
    finish_far(0)
    pump(1, 1)
    tiles(far_x)
    pump(1, 2)

    scaled = []
    cw = width // c_chunks

    def chain_copy(j):
        cols = pl.ds(j * cw, cw)
        return remote(
            snd.at[:, cols], car.at[:, cols], c_send.at[j], c_recv.at[j],
            {"sp": jnp.minimum(z + 1, n_sp - 1)},
        )

    def chain_first(j):
        cols = pl.ds(j * cw, cw)

        @pl.when(z == 0)
        def _():
            car[:, cols] = jnp.zeros((N, cw), BF16)
            snd[:, cols] = st[:, cols].astype(BF16)
            chain_copy(j).start()

    def chain(j):
        @pl.when(z > 0)
        def _():
            chain_copy(j).wait_recv()

            @pl.when(z < n_sp - 1)
            def _():
                for p in range(j * cw // (2 * P_SIZE), (j + 1) * cw // (2 * P_SIZE)):
                    pc = pair_cols(p)
                    total = spread(whole, p, first_row) * car[:, pc].astype(F32) + st[:, pc]
                    snd[:, pc] = total.astype(BF16)
                chain_copy(j).start()

    def inner(g):
        cb = dot(cm[:, g * N : (g + 1) * N], bm[:, g * N : (g + 1) * N], ((1,), (1,)))
        for p in range(g * per_group // 2, (g + 1) * per_group // 2):
            parts = []
            for h in (2 * p, 2 * p + 1):
                gap = jnp.where(lower, cum[:, h : h + 1] - cum_t[h : h + 1, :], -jnp.inf)
                parts.append(dot((cb * jnp.exp(gap)).astype(BF16), scaled[p]))
            bypass = spread(skip_ref[...], p, first_row) * xs[:, pair_cols(p)].astype(F32)
            y[:, pair_cols(p)] = jnp.where(first_head, parts[0], parts[1]) + bypass

    def local_state(g):
        for p in range(g * per_group // 2, (g + 1) * per_group // 2):
            xp = xs[:, pair_cols(p)].astype(F32)
            part = (xp * spread(step, p, first_head)).astype(BF16)
            sc[:, pair_cols(p)] = (part.astype(F32) * spread(to_end, p, first_head)).astype(BF16)
            scaled.append(part)
        cols = pl.ds(g * gw, gw)
        st[:, cols] = dot(bm[:, g * N : (g + 1) * N], sc[:, cols], ((0,), (0,)))
        for j in range(g * c_chunks // G, (g + 1) * c_chunks // G):
            chain_first(j)

    def chain_slot(slot):
        @pl.when(jnp.minimum(z, 3) == slot)
        def _():
            for j in range(c_chunks):
                chain(j)

    for g in range(G):
        local_state(g)
    pump(1, 3)
    pump(2, 0)
    inner(0)
    pump(1, 4)
    chain_slot(1)
    pump(2, 1)
    inner(1)
    pump(2, 2)
    chain_slot(2)
    finish_near(1)
    tiles(near_z)
    finish_far(1)
    tiles(far_z)
    chain_slot(3)

    for g in range(G):
        cols = pl.ds(g * gw, gw)
        reached = dot(cm[:, g * N : (g + 1) * N], car[:, cols])
        gate = px[pl.ds(0, tok), cols]
        square = jnp.zeros((tok, 1), F32)
        first = g * per_group // 2
        for p in range(first, first + per_group // 2):
            here = slice((p - first) * 2 * P_SIZE, (p - first + 1) * 2 * P_SIZE)
            mixed = y[:, pair_cols(p)] + spread(reach, p, first_head) * reached[:, here]
            gated = mixed.astype(BF16).astype(F32) * gate[:, here]
            square = square + jnp.sum(gated * gated, axis=1, keepdims=True)
            y[:, pair_cols(p)] = gated
        inv = lax.rsqrt(square * (1.0 / gw) + EPSILON)
        nrm[:, cols] = (y[:, cols] * inv * scale_ref[:, cols]).astype(BF16)

    fw = wf.shape[2]

    def finish_output(d):
        part = pl.ds(pl.multiple_of(d * fw, 128), fw)
        out_ref[:, part] = dot(nrm[...], wf[d]).astype(BF16)
        pltpu.make_async_copy(out_ref.at[:, part], out_hbm.at[:, part], o_sem.at[d]).start()

    pump(2, 3)
    finish_near(2)
    finish_output(dp)
    finish_output(dp + 1 - 2 * core)
    pump(2, 4)
    for o in range(1, n_x):
        finish_output(owner_of(o))
    finish_far(2)
    for o in range(1, n_x):
        finish_output(owner_of(o) + 1 - 2 * core)
    for d in range(n_dp):
        part = pl.ds(d * fw, fw)
        pltpu.make_async_copy(out_ref.at[:, part], out_hbm.at[:, part], o_sem.at[d]).wait()

    for copy in sends:
        copy.wait_send()

    @pl.when(z < n_sp - 1)
    def _():
        halo_copy().wait_send()
        for j in range(c_chunks):
            chain_copy(j).wait_send()


def shards(
    dims,
    mixer_source_array,
    source_projection,
    gating_projection,
    entry_mapping_projection,
    readout_mapping_projection,
    increment_projection,
    source_conv_taps,
    entry_mapping_taps,
    readout_mapping_taps,
    increment_offsets,
    channel_damping_rate,
    bypass_coefficients,
    stride_multiplier,
    added_log_damping,
    norm_scale_factor,
    final_projection,
):
    n_grp, n_sp, n_dp, c_chunks = dims
    n_x = n_dp // 2
    hidden = mixer_source_array[0]
    tok, model = hidden.shape
    width = source_projection.shape[1]
    gn = G * N
    out_width = final_projection.shape[1] * n_dp
    dma = pltpu.SemaphoreType.DMA
    remote_srcs = max(n_x - 1, 1)
    vmem = pl.BlockSpec(memory_space=pltpu.VMEM)
    hbm = pl.BlockSpec(memory_space=pl.ANY)
    output = pl.pallas_call(
        functools.partial(kernel, dims),
        out_shape=jax.ShapeDtypeStruct((tok, out_width), BF16),
        in_specs=[hbm] * 7 + [vmem] * 9,
        out_specs=hbm,
        scratch_shapes=[
            pltpu.VMEM((HALO + tok, model), BF16),
            pltpu.VMEM((model, width), BF16),
            pltpu.VMEM((model, width), BF16),
            pltpu.VMEM((n_dp,) + final_projection.shape, BF16),
            pltpu.VMEM((HALO + tok, 2 * gn), F32),
            pltpu.VMEM((HALO + tok, width), F32),
            pltpu.VMEM((tok, gn), BF16),
            pltpu.VMEM((tok, gn), BF16),
            pltpu.VMEM((tok, width), BF16),
            pltpu.VMEM((tok, width), BF16),
            pltpu.VMEM((tok, width), F32),
            pltpu.VMEM((N, width), F32),
            pltpu.VMEM((N, width), BF16),
            pltpu.VMEM((N, width), BF16),
            pltpu.VMEM((tok, width), BF16),
            pltpu.VMEM((tok, out_width), BF16),
            pltpu.VMEM((model, 2 * gn), BF16),
            pltpu.VMEM((increment_projection.shape[1], model), BF16),
            dma((7,)),
            dma,
            dma,
            dma((3, remote_srcs, 3)),
            dma((3, remote_srcs, 3)),
            dma((3, remote_srcs, 3)),
            dma((3, remote_srcs, 3)),
            dma((3, remote_srcs, 2)),
            dma((3, remote_srcs, 2)),
            dma((3, n_x, 4)),
            dma((3, 2)),
            dma((c_chunks,)),
            dma((c_chunks,)),
            dma((n_dp,)),
        ],
        compiler_params=pltpu.CompilerParams(
            collective_id=0, has_side_effects=True, vmem_limit_bytes=56 * 1024 * 1024
        ),
    )(
        hidden,
        source_projection,
        gating_projection,
        final_projection,
        entry_mapping_projection,
        readout_mapping_projection,
        increment_projection.T,
        source_conv_taps,
        entry_mapping_taps,
        readout_mapping_taps,
        increment_offsets[None],
        channel_damping_rate[None],
        bypass_coefficients[None],
        stride_multiplier,
        jnp.swapaxes(added_log_damping, 1, 2),
        norm_scale_factor[None],
    )
    return output[None]


def solution(mesh):
    n_grp, n_sp, n_dp = (mesh.shape[a] for a in ("grp", "sp", "dp"))
    return jax.shard_map(
        functools.partial(shards, (n_grp, n_sp, n_dp, 8)),
        mesh=mesh,
        in_specs=(
            P(("grp", "dp"), "sp", None),
            P("dp", None),
            P("dp", None),
            P(),
            P(),
            P(),
            P(),
            P(),
            P(),
            P(),
            P(),
            P(),
            P(("grp", "dp"), None),
            P(("grp", "dp"), None, None),
            P(),
            P(None, "dp"),
        ),
        out_specs=P(("grp", "dp"), "sp", None),
        check_vma=False,
    )
```

profile of v0, /device:TPU:25, one launch (start us, length us, event | category | flops | bytes accessed | tf_op | source)
XLA Modules:
  0.0 46.1 jit_solution(9254576028260222316)
XLA Ops:
  0.0 44.0 %shard_map.154 = bf16[192,2048]{1,0:T(8,128)(2,1)} custom-call(bf16[192,2048]{1,0:T(8,128)(2,1)} %bitcast.9, bf16[512,1024]{1,0:T(8,128)(2,1)} %wx_hbm.1, bf16[512,1024]{1,0:T(8,128)(2,1)} %wz_hbm.1, bf16[1024,512]{1,0:T(8,128)(2,1)} %wf_hbm.1, bf16[2048,256]{1,0:T(8,128)(2,1)} %wb_hbm.1, bf16[2048,256]{1,0:T(8,128)(2,1)} %wc_hbm.1, ...), custom_call_target="tpu_custom_call" | custom-call | tf_op jit(solution)/shard_map/pallas_call | solution.py:491
  44.0 2.1 %copy.18 = bf16[1,192,2048]{2,1,0:T(8,128)(2,1)} copy(bf16[1,192,2048]{2,1,0:T(8,128)(2,1)} %bitcast.8) | data formatting | bytes 1572864
where the time goes:
time: 46.3 us; the launch traced here: 46.1 us
  Pallas kernels  44 us (95%)
  local copies, waits for them, and re-layouts  2.09 us (5%)
    pallas_call x1, Pallas kernels, shards(): pl.pallas_call(functools.partial(kernel, dims), out_shape=jax.ShapeDtypeS...  44 us
    unnamed x1, local copies, waits for them, and re-layouts  2.09 us

commit v1 on v0

v1 whole, which is shorter than its diff:
```python
import functools

import jax
import jax.numpy as jnp
from jax import lax
from jax.experimental import pallas as pl
from jax.experimental.pallas import tpu as pltpu
from jax.sharding import PartitionSpec as P

P_SIZE = 64
N = 128
G = 2
CONV_W = 4
EPSILON = 1e-06
HIGH = lax.Precision.HIGHEST
MESH = pl.DeviceIdType.MESH
HALO = 16
CHUNKS = (128, 256, 128)
TYPES = (2, 2, 4, 4, 3, 4, 3, 4, 2, 4)
X_ORDER = (("S", 0), ("S", 3), ("S", 1), ("S", 2), ("E", 3), ("S", 4), ("E", 2), ("S", 8), ("S", 5), ("S", 6), ("E", 4), ("S", 7), ("E", 5), ("S", 9), ("E", 6), ("E", 9), ("E", 7))
ORDER = (
    ("seeds", 0),
    ("seeds", 3),
    "pbc",
    "nearz",
    ("relay0", 0),
    ("relay1", 0),
    ("seeds", 1),
    ("seeds", 2),
    "nearx",
    ("farx", 3),
    ("state", 3),
    ("relay0", 1),
    ("farx", 0),
    ("relay1", 1),
    ("state", 0),
    ("inner", 3),
    ("seeds", 4),
    ("farx", 2),
    ("state", 2),
    ("farx", 1),
    ("state", 1),
    ("seeds", 8),
    ("inner", 1),
    ("relay0", 4),
    ("inner", 0),
    ("seeds", 5),
    ("relay1", 8),
    ("farz", 4),
    ("relay0", 8),
    ("seeds", 6),
    ("seeds", 7),
    ("inner", 2),
    ("farz", 5),
    ("seeds", 9),
    "finish",
    ("relay0", 6),
    "outn",
    ("out", 8),
    ("out", 9),
    ("out", 7),
    ("out", 6),
)
SLOTS = (
    ((0, 30), (1, 30), (2, 28), (3, 29)),
    ((0, 18), (1, 26), (2, 24), (3, 15)),
    ((0, 24), (1, 29), (2, 27), (3, 22)),
    ((0, 30), (1, 34), (2, 34), (3, 33)),
)


def plan(n_sp, n_x, gw, fw):
    steps = []
    for w, wide in enumerate((gw, gw, fw)):
        cw = min(CHUNKS[w], wide)
        steps += [(w, j, cw) for j in range(wide // cw)]
    if (n_sp, n_x, len(steps)) == (4, 2, len(TYPES)):
        return steps, TYPES, X_ORDER, ORDER, SLOTS
    every = range(len(steps))
    x_order = [(kind, s) for s in every for kind in "SE"]
    order = ["nearz", "pbc", "nearx"]
    for s in every:
        if steps[s][0] == 2 and "outn" not in order:
            order += ["finish", "outn"]
        order += [("seeds", s), ("relay0", s)]
        order += [[("farx", s), ("state", s), ("inner", s)], [("farz", s)], [("out", s)]][steps[s][0]]
    slots = [[(s, order.index("finish")) for s in every if steps[s][0] == 0]] * 4
    return steps, [3] * len(steps), x_order, order, slots
F32 = jnp.float32
BF16 = jnp.bfloat16


def dot(a, b, dims=((1,), (0,)), precision=None):
    return lax.dot_general(a, b, (dims, ((), ())), precision=precision, preferred_element_type=F32)


def silu(v):
    return v * (1.0 / (1.0 + jnp.exp(-v)))


def kernel(
    dims,
    x_hbm,
    wx_hbm,
    wz_hbm,
    wf_hbm,
    wb_hbm,
    wc_hbm,
    wdt_hbm,
    tx_hbm,
    tb_hbm,
    tc_hbm,
    off_hbm,
    rate_hbm,
    skip_hbm,
    stride_hbm,
    damp_hbm,
    scale_hbm,
    out_ref,
    xe,
    wx,
    wz,
    wf,
    wbc,
    wdt,
    tx,
    tb,
    tc,
    off,
    rate,
    skip,
    stride,
    damp,
    scale,
    pbc,
    px,
    pcx,
    gz,
    bm,
    cm,
    cb,
    xs,
    scl,
    sc,
    y,
    st,
    car,
    snd,
    nrm,
    oth,
    loc_sem,
    p_send,
    p_recv,
    link_send,
    seed_recv,
    rest_recv,
    relay_recv,
    c_recv,
    n_recv,
    o_recv,
):
    n_grp, n_sp, n_dp = dims
    n_x = n_dp // 2
    grp, z, dp = (lax.axis_index(a) for a in ("grp", "sp", "dp"))
    xi, core = dp // 2, dp % 2
    tok = out_ref.shape[0]
    heads = off.shape[1]
    per_group = heads // G
    gw = xs.shape[1]
    rows_dev = wx_hbm.shape[0]
    fw = wf_hbm.shape[1]
    width = wf_hbm.shape[0]
    halo_send, x_send, y_send, z_send, c_send, n_send, o_send = (link_send.at[i] for i in range(7))
    halo_recv = p_recv.at[5]
    own_cols = pl.ds(pl.multiple_of(core * gw, 128), gw)
    other_cols = pl.ds(pl.multiple_of((1 - core) * gw, 128), gw)
    partner = {"dp": xi * 2 + 1 - core}
    y_peer = {"grp": 1 - grp}
    zb = z % 2
    z_peer = {"sp": z + 1 - 2 * zb}
    bufs = (wx, wz, wf)
    srcs = (wx_hbm, wz_hbm, wf_hbm)
    own_q = grp * 2 + zb
    y_q = (1 - grp) * 2 + zb
    z_q = grp * 2 + 1 - zb
    far_q = (1 - grp) * 2 + 1 - zb

    barrier = pltpu.get_barrier_semaphore()

    def greet(peer):
        pl.semaphore_signal(barrier, inc=1, device_id=peer, device_id_type=MESH)

    greet(partner)
    greet(y_peer)
    for o in range(1, n_x):
        for d in range(2):
            greet({"dp": lax.rem(xi + o, n_x) * 2 + d})

    @pl.when(z > 0)
    def _():
        for d in range(2):
            greet({"sp": z - 1, "dp": xi * 2 + d})

    @pl.when(z < n_sp - 1)
    def _():
        for d in range(2):
            greet({"sp": z + 1, "dp": xi * 2 + d})

    def remote(src, dst, send, recv, peer):
        return pltpu.make_async_remote_copy(
            src_ref=src, dst_ref=dst, send_sem=send, recv_sem=recv,
            device_id=peer, device_id_type=MESH,
        )

    locals_ = []

    def local(src, dst):
        copy = pltpu.make_async_copy(src, dst, loc_sem.at[len(locals_)])
        copy.start()
        locals_.append(copy)
        return copy

    def far_rows(chip):
        return pl.ds(pl.multiple_of(chip * width, 128), width)

    def seq_rows(s):
        return pl.ds(s * tok, tok)

    dyn_rows = pl.ds(pl.multiple_of(core * tok, 16), tok)
    head_rows = pl.ds(pl.multiple_of(core * per_group, 8), per_group)
    other_heads = pl.ds(pl.multiple_of((1 - core) * per_group, 8), per_group)
    dev_rows = pl.ds(pl.multiple_of(dp * rows_dev, 16), rows_dev)
    partner_rows = pl.ds(pl.multiple_of((xi * 2 + 1 - core) * rows_dev, 16), rows_dev)
    group_n = pl.ds(pl.multiple_of(core * N, 128), N)

    small = [local(x_hbm, xe.at[dyn_rows])]
    small += [local(stride_hbm, stride.at[core]), local(damp_hbm.at[0, head_rows], damp.at[core])]
    small += [local(wdt_hbm, wdt), local(off_hbm, off), local(rate_hbm, rate)]
    maps = [local(wb_hbm.at[:, group_n], wbc.at[:, pl.ds(0, N)])]
    maps += [local(wc_hbm.at[:, group_n], wbc.at[:, pl.ds(N, N)])]
    maps += [local(tb_hbm.at[:, group_n], tb), local(tc_hbm.at[:, group_n], tc)]
    own = [local(srcs[w].at[:, own_cols], bufs[w].at[dev_rows]) for w in range(2)]
    own += [local(wf_hbm, wf.at[far_rows(xi)])]
    late = [local(tx_hbm.at[:, own_cols], tx), local(skip_hbm, skip), local(scale_hbm.at[:, own_cols], scale)]

    greeted = 2 + 2 * (n_x - 1) + 2 * jnp.minimum(z, 1) + 2 * jnp.minimum(n_sp - 1 - z, 1)
    pl.semaphore_wait(barrier, greeted)

    steps, types, x_order, order, slots = plan(n_sp, n_x, gw, fw)
    last_step = len(steps) - 1
    direct, relayed = [], []
    for kind in types:
        turn = sum(1 for d in direct if len(d) == 1) % 2
        direct.append({2: (), 3: (turn,), 4: (0, 1)}[kind])
        relayed.append(tuple(k for k in (0, 1) if k not in direct[-1]))

    def piece_rows(s):
        return width // 8 if steps[s][0] == 2 else rows_dev // 4

    def place(s, chip, q, k):
        w, j, cw = steps[s]
        size = piece_rows(s)
        row = chip * width + (q * 2 + k) * size if w == 2 else (chip * 2 + k) * rows_dev + q * size
        return bufs[w].at[pl.ds(pl.multiple_of(row, 16), size), pl.ds(j * cw, cw)]

    def origin(s, q, k, d):
        w, j, cw = steps[s]
        size = piece_rows(s)
        row, col = ((q * 2 + k) * size, j * cw) if w == 2 else (q * size, d * gw + j * cw)
        return srcs[w].at[pl.ds(pl.multiple_of(row, 16), size), pl.ds(pl.multiple_of(col, 128), cw)]

    def owner_of(o):
        return lax.rem(xi - o + n_x, n_x)

    sent = {"x": [0, 0], "y": 0, "z": 0}

    def x_start(s, o, q, k, d, recv):
        peer = {"dp": lax.rem(xi + o, n_x) * 2 + d}
        remote(origin(s, q, k, d), place(s, xi, q, k), x_send, recv.at[s], peer).start()

    def unit(s):
        return piece_rows(s) * steps[s][2] // gw

    def x_seeds(s):
        for o in range(1, n_x):
            if steps[s][0] == 2:
                for k in range(2):
                    x_start(s, o, own_q, k, core, seed_recv)
            else:
                for d in (core, 1 - core):
                    x_start(s, o, own_q, core, d, seed_recv)
            for k in range(2):
                sent["x"][k] += 2 * unit(s)

    def x_extras(s):
        for o in range(1, n_x):
            if steps[s][0] == 2:
                for k in direct[s]:
                    x_start(s, o, far_q, k, core, rest_recv)
                    sent["x"][0] += unit(s)
                    sent["x"][1] += unit(s)
            elif len(direct[s]) == 2:
                for d in (core, 1 - core):
                    x_start(s, o, far_q, core, d, rest_recv)
                sent["x"][0] += 2 * unit(s)
                sent["x"][1] += 2 * unit(s)
            else:
                for k in direct[s]:
                    sent["x"][k] += 2 * unit(s)

                    @pl.when(core == k)
                    def _(k=k, o=o):
                        for d in (core, 1 - core):
                            x_start(s, o, far_q, k, d, rest_recv)

    def y_start(s, o, q, k):
        spot = place(s, owner_of(o), q, k)
        remote(spot, spot, y_send, rest_recv.at[s], y_peer).start()
        sent["y"] += unit(s)

    def z_start(s, o, k):
        spot = place(s, owner_of(o), own_q, k)
        recv = relay_recv.at[s, k] if k in relayed[s] else rest_recv.at[s]
        remote(spot, spot, z_send, recv, z_peer).start()
        sent["z"] += unit(s)

    def pieces_wait(s, count, recv):
        w, j, cw = steps[s]
        spot = bufs[w].at[pl.ds(0, count * (n_x - 1) * piece_rows(s)), pl.ds(j * cw, cw)]
        remote(spot, spot, x_send, recv, partner).wait_recv()

    def halo_copies():
        up = jnp.minimum(z + 1, n_sp - 1)
        dst = xe.at[pl.ds(pl.multiple_of(2 * tok + core * HALO, 16), HALO)]
        src = x_hbm.at[pl.ds(tok - HALO, HALO)]
        return [remote(src, dst, halo_send, halo_recv, {"sp": up, "dp": xi * 2 + d}) for d in (core, 1 - core)]

    @pl.when(z < n_sp - 1)
    def _():
        for copy in halo_copies():
            copy.start()

    sends = []

    def start(copy):
        copy.start()
        sends.append(copy)

    for n, (kind, s) in enumerate(x_order):
        (x_seeds if kind == "S" else x_extras)(s)
        if n == 0:
            start(remote(x_hbm, xe.at[dyn_rows], p_send.at[0], p_recv.at[0], partner))
            start(remote(stride_hbm, stride.at[core], p_send.at[1], p_recv.at[1], partner))
            start(remote(damp_hbm.at[0, other_heads], damp.at[core], p_send.at[2], p_recv.at[2], partner))
            for w in range(2):
                start(remote(srcs[w].at[:, other_cols], bufs[w].at[dev_rows], p_send.at[3 + w], p_recv.at[3 + w], partner))

    def seeds(s):
        pieces_wait(s, 2, seed_recv.at[s])
        for o in range(1, n_x):
            for k in relayed[s] + direct[s]:
                z_start(s, o, k)
            for k in range(2):
                y_start(s, o, own_q, k)

    def relay(s, r):
        k = relayed[s][r]
        pieces_wait(s, 1, relay_recv.at[s, k])
        for o in range(1, n_x):
            y_start(s, o, z_q, k)

    def rest(s):
        pieces_wait(s, 6 - len(relayed[s]), rest_recv.at[s])

    depth = 2 * rows_dev

    def chip_rows(o):
        return pl.ds(pl.multiple_of(owner_of(o) * depth, 128), depth)

    def square_iota(size):
        return [lax.broadcasted_iota(jnp.int32, (size, size), d) for d in (0, 1)]

    def pick(values, axis):
        low, high = (lax.slice_in_dim(values, i * per_group, (i + 1) * per_group, axis=axis) for i in range(2))
        return jnp.where(core == 0, low, high)

    def column(ref):
        i, j = square_iota(heads)
        mine = pick(jnp.sum(jnp.where(i == j, ref[...], 0.0), axis=1, keepdims=True), 0)
        return jnp.concatenate([mine, mine], axis=0)

    def my_positions(values):
        mine = values[:, 0:tok]
        for i in range(1, n_sp):
            mine = jnp.where(z == i, values[:, i * tok : (i + 1) * tok], mine)
        return mine

    for copy in small:
        copy.wait()
    other_seq = xe.at[pl.ds(pl.multiple_of((1 - core) * tok, 16), tok)]
    remote(x_hbm, other_seq, p_send.at[0], p_recv.at[0], partner).wait_recv()
    remote(stride_hbm, stride.at[1 - core], p_send.at[1], p_recv.at[1], partner).wait_recv()
    remote(damp_hbm.at[0, other_heads], damp.at[1 - core], p_send.at[2], p_recv.at[2], partner).wait_recv()

    raw = [pick(dot(wdt[...], xe[seq_rows(s), :], ((1,), (1,))), 0) for s in range(2)]
    raw = jnp.concatenate(raw, axis=0).astype(BF16).astype(F32)
    pre = raw + column(off)
    step_t = jnp.maximum(pre, 0.0) + jnp.log1p(jnp.exp(-jnp.abs(pre)))
    tempo = [jnp.broadcast_to(my_positions(stride[s]), (per_group, tok)) for s in range(2)]
    extra = [my_positions(damp[s]) for s in range(2)]
    keep = -column(rate) * step_t * jnp.concatenate(tempo, axis=0) + jnp.concatenate(extra, axis=0)
    row, col = square_iota(tok)
    lower = row >= col
    step = dot((row == col).astype(F32), step_t, ((1,), (1,)), HIGH)
    cum = dot(lower.astype(F32), keep, ((1,), (1,)), HIGH)
    cum_t = dot(keep, (row <= col).astype(F32), precision=HIGH)
    last = cum[tok - 1 : tok, :]
    to_end = jnp.exp(last - cum)
    reach = jnp.exp(cum)
    whole = jnp.exp(last)
    first_head = lax.broadcasted_iota(jnp.int32, (tok, 2 * P_SIZE), 1) < P_SIZE
    first_row = first_head[0:1, :]

    def spread(values, p, mask):
        return jnp.where(mask, values[:, 2 * p : 2 * p + 1], values[:, 2 * p + 1 : 2 * p + 2])

    def pair_cols(p):
        return pl.ds(p * 2 * P_SIZE, 2 * P_SIZE)

    pairs = per_group // 2
    main = pl.ds(0, 2 * tok)
    span = HALO + tok

    def near(w):
        own[w].wait()
        spot = bufs[w].at[partner_rows]
        remote(spot, spot, p_send.at[3 + w], p_recv.at[3 + w], partner).wait_recv()

    def tiles(width, tile, body):
        def run(j, carry):
            body(pl.ds(pl.multiple_of(j * tile, tile), tile))
            return carry

        lax.fori_loop(0, width // tile, run, 0)

    def near_z(cols):
        gz[:, cols] = dot(xe[main, chip_rows(0)], wz[chip_rows(0), cols])

    def put(buf, cols, values):
        for s in range(2):
            buf[pl.ds(s * span, HALO), cols] = values[2 * tok + s * HALO : 2 * tok + (s + 1) * HALO, :]
            buf[pl.ds(s * span + HALO, tok), cols] = values[s * tok : (s + 1) * tok, :]

    def conv(buf, s, cols, taps):
        first = s * span + HALO - CONV_W + 1
        total = taps[0:1, :] * buf[pl.ds(first, tok), cols]
        for k in range(1, CONV_W):
            total = total + taps[k : k + 1, :] * buf[pl.ds(first + k, tok), cols]
        return silu(total).astype(BF16)

    skip_vals = []

    def near_x(cols):
        px[:, cols] = dot(xe[:, chip_rows(0)], wx[chip_rows(0), cols])

    def maps_task():
        @pl.when(z == 0)
        def _():
            xe[pl.ds(2 * tok, 2 * HALO), :] = jnp.zeros((2 * HALO, xe.shape[1]), BF16)

        @pl.when(z > 0)
        def _():
            spot = xe.at[pl.ds(2 * tok, 2 * HALO)]
            remote(spot, spot, halo_send, halo_recv, partner).wait_recv()

        for copy in maps:
            copy.wait()
        put(pbc, pl.ds(0, 2 * N), dot(xe[...], wbc[...]).astype(BF16).astype(F32))
        for s in range(2):
            bm[seq_rows(s), :] = conv(pbc, s, pl.ds(0, N), tb[...])
            cm[seq_rows(s), :] = conv(pbc, s, pl.ds(N, N), tc[...])
        for s in range(2):
            cb[s] = dot(cm[seq_rows(s), :], bm[seq_rows(s), :], ((1,), (1,)))
        for copy in late:
            copy.wait()
        skip_vals.append(pick(skip[...], 1))

    def far_x(cols):
        acc = px[:, cols]
        for o in range(1, n_x):
            acc = acc + dot(xe[:, chip_rows(o)], wx[chip_rows(o), cols])
        put(pcx, cols, acc.astype(BF16).astype(F32))
        for s in range(2):
            xs[seq_rows(s), cols] = conv(pcx, s, cols, tx[:, cols])

    def far_z(cols):
        acc = gz[:, cols]
        for o in range(1, n_x):
            acc = acc + dot(xe[main, chip_rows(o)], wz[chip_rows(o), cols])
        gz[:, cols] = silu(acc.astype(BF16).astype(F32))

    def chain_copy(s, p):
        pc = pair_cols(p)
        return remote(
            snd.at[s, :, pc], car.at[s, :, pc], c_send, c_recv.at[s, p],
            {"sp": jnp.minimum(z + 1, n_sp - 1)},
        )

    def step_pairs(cols):
        return range(cols.start // (2 * P_SIZE), (cols.start + cols.size) // (2 * P_SIZE))

    def local_state(cols):
        for s in range(2):
            for p in step_pairs(cols):
                pc = pair_cols(p)
                v = s * pairs + p
                part = (xs[seq_rows(s), pc].astype(F32) * spread(step, v, first_head)).astype(BF16)
                scl[seq_rows(s), pc] = part
                sc[seq_rows(s), pc] = (part.astype(F32) * spread(to_end, v, first_head)).astype(BF16)
            st[s, :, cols] = dot(bm[seq_rows(s), :], sc[seq_rows(s), cols], ((0,), (0,)))

        @pl.when(z == 0)
        def _():
            for s in range(2):
                car[s, :, cols] = jnp.zeros((N, cols.size), BF16)
                for p in step_pairs(cols):
                    pc = pair_cols(p)
                    snd[s, :, pc] = st[s, :, pc].astype(BF16)
                    chain_copy(s, p).start()

    def chain(cols):
        for s in range(2):
            for p in step_pairs(cols):
                chain_copy(s, p).wait_recv()

                @pl.when(z < n_sp - 1)
                def _(s=s, p=p):
                    pc = pair_cols(p)
                    v = s * pairs + p
                    total = spread(whole, v, first_row) * car[s, :, pc].astype(F32) + st[s, :, pc]
                    snd[s, :, pc] = total.astype(BF16)
                    chain_copy(s, p).start()

    def chain_slot(slot, cols):
        @pl.when(jnp.minimum(z, 3) == slot)
        def _():
            chain(cols)

    def inner(s, cols):
        for p in step_pairs(cols):
            pc = pair_cols(p)
            parts = []
            for v in (s * per_group + 2 * p, s * per_group + 2 * p + 1):
                gap = jnp.where(lower, cum[:, v : v + 1] - cum_t[v : v + 1, :], -jnp.inf)
                parts.append(dot((cb[s] * jnp.exp(gap)).astype(BF16), scl[seq_rows(s), pc]))
            bypass = spread(skip_vals[0], p, first_row) * xs[seq_rows(s), pc].astype(F32)
            y[seq_rows(s), pc] = jnp.where(first_head, parts[0], parts[1]) + bypass

    def step_cols(s):
        return pl.ds(steps[s][1] * steps[s][2], steps[s][2])

    def slot_rows(s, swap):
        return pl.ds(pl.multiple_of(lax.rem(s + core + swap, 2) * tok, 16), tok)

    def finish(s):
        reached = dot(cm[seq_rows(s), :], car[s])
        square = jnp.zeros((tok, 1), F32)
        for p in range(pairs):
            pc = pair_cols(p)
            here = slice(p * 2 * P_SIZE, (p + 1) * 2 * P_SIZE)
            mixed = y[seq_rows(s), pc] + spread(reach, s * pairs + p, first_head) * reached[:, here]
            gated = mixed.astype(BF16).astype(F32) * gz[seq_rows(s), pc]
            square = square + jnp.sum(gated * gated, axis=1, keepdims=True)
            y[seq_rows(s), pc] = gated
        inv = lax.rsqrt(square * (1.0 / gw) + EPSILON)
        nrm[slot_rows(s, 0), own_cols] = (y[seq_rows(s), :] * inv * scale[...]).astype(BF16)
        remote(
            nrm.at[slot_rows(s, 0), own_cols], nrm.at[slot_rows(s, 1), own_cols],
            n_send, n_recv.at[0], partner,
        ).start()

    def out_cols(o, s, d):
        cols = step_cols(s)
        return pl.ds(pl.multiple_of((owner_of(o) * 2 + d) * fw + cols.start, 128), cols.size)

    def out_copy(o, s, d):
        cols = step_cols(s)
        return remote(
            oth.at[:, pl.ds(o * fw + cols.start, cols.size)], out_ref.at[:, out_cols(o, s, d)],
            o_send, o_recv.at[0], partner,
        )

    def output(o, s):
        cols = step_cols(s)
        part = dot(nrm[...], wf[far_rows(owner_of(o)), cols]).astype(BF16)
        out_ref[:, out_cols(o, s, core)] = part[0:tok, :]
        oth[:, pl.ds(o * fw + cols.start, cols.size)] = part[tok : 2 * tok, :]
        out_copy(o, s, core).start()

    f_steps = [s for s in range(len(steps)) if steps[s][0] == 2]

    def out_near():
        own[2].wait()
        spot = nrm.at[:, other_cols]
        remote(spot, spot, n_send, n_recv.at[0], partner).wait_recv()
        for s in f_steps:
            output(0, s)

    def run(name):
        if name == "nearz":
            near(1)
            tiles(gw, 256, near_z)
        elif name == "pbc":
            maps_task()
        elif name == "nearx":
            near(0)
            tiles(gw, 256, near_x)
        elif name == "finish":
            for s in range(2):
                finish(s)
        elif name == "outn":
            out_near()
        else:
            task, s = name
            cols = step_cols(s)
            if task == "seeds":
                seeds(s)
            elif task in ("relay0", "relay1"):
                relay(s, int(task[-1]))
            elif task == "farx":
                rest(s)
                far_x(cols)
            elif task == "state":
                local_state(cols)
            elif task == "inner":
                for q in range(2):
                    inner(q, cols)
            elif task == "farz":
                rest(s)
                far_z(cols)
            else:
                rest(s)
                for o in range(1, n_x):
                    output(o, s)

    for n, name in enumerate(order):
        for level in (1, 2, 3):
            for s, at in slots[level]:
                if at == n:
                    chain_slot(level, step_cols(s))
        run(name)
    remote(oth, oth, o_send, o_recv.at[0], partner).wait_recv()

    def sent_wait(send, rows):
        if rows:
            spot = wx.at[pl.ds(0, rows)]
            remote(spot, spot, send, n_recv.at[0], partner).wait_send()

    for copy in sends:
        copy.wait_send()
    sent_wait(y_send, sent["y"])
    sent_wait(z_send, sent["z"])
    if sent["x"][0] == sent["x"][1]:
        sent_wait(x_send, sent["x"][0])
    else:
        for k in range(2):

            @pl.when(core == k)
            def _(k=k):
                sent_wait(x_send, sent["x"][k])

    spot = nrm.at[:, own_cols]
    remote(spot, spot, n_send, n_recv.at[0], partner).wait_send()
    remote(oth, oth, o_send, o_recv.at[0], partner).wait_send()

    @pl.when(z < n_sp - 1)
    def _():
        spot = xe.at[pl.ds(2 * tok, 2 * HALO)]
        remote(spot, spot, halo_send, halo_recv, partner).wait_send()
        remote(snd, snd, c_send, n_recv.at[0], partner).wait_send()


def shards(
    dims,
    mixer_source_array,
    source_projection,
    gating_projection,
    entry_mapping_projection,
    readout_mapping_projection,
    increment_projection,
    source_conv_taps,
    entry_mapping_taps,
    readout_mapping_taps,
    increment_offsets,
    channel_damping_rate,
    bypass_coefficients,
    stride_multiplier,
    added_log_damping,
    norm_scale_factor,
    final_projection,
):
    n_grp, n_sp, n_dp = dims
    n_x = n_dp // 2
    hidden = mixer_source_array[0]
    tok, model = hidden.shape
    width = source_projection.shape[1]
    gw = width // G
    heads = increment_projection.shape[1]
    fw = final_projection.shape[1]
    length = stride_multiplier.shape[1]
    out_width = fw * n_dp
    n_steps = len(plan(n_sp, n_x, gw, fw)[0])
    span = HALO + tok
    dma = pltpu.SemaphoreType.DMA
    hbm = pl.BlockSpec(memory_space=pl.ANY)
    output = pl.pallas_call(
        functools.partial(kernel, dims),
        out_shape=pltpu.VMEM((tok, out_width), BF16),
        in_specs=[hbm] * 16,
        out_specs=pl.BlockSpec(memory_space=pltpu.VMEM),
        scratch_shapes=[
            pltpu.VMEM((2 * span, model), BF16),
            pltpu.VMEM((model, gw), BF16),
            pltpu.VMEM((model, gw), BF16),
            pltpu.VMEM((n_x * width, fw), BF16),
            pltpu.VMEM((model, 2 * N), BF16),
            pltpu.VMEM((heads, model), BF16),
            pltpu.VMEM((CONV_W, gw), F32),
            pltpu.VMEM((CONV_W, N), F32),
            pltpu.VMEM((CONV_W, N), F32),
            pltpu.VMEM((1, heads), F32),
            pltpu.VMEM((1, heads), F32),
            pltpu.VMEM((1, heads), F32),
            pltpu.VMEM((2, 1, length), F32),
            pltpu.VMEM((2, heads // G, length), F32),
            pltpu.VMEM((1, gw), F32),
            pltpu.VMEM((2 * span, 2 * N), F32),
            pltpu.VMEM((2 * span, gw), F32),
            pltpu.VMEM((2 * span, gw), F32),
            pltpu.VMEM((2 * tok, gw), F32),
            pltpu.VMEM((2 * tok, N), BF16),
            pltpu.VMEM((2 * tok, N), BF16),
            pltpu.VMEM((2, tok, tok), F32),
            pltpu.VMEM((2 * tok, gw), BF16),
            pltpu.VMEM((2 * tok, gw), BF16),
            pltpu.VMEM((2 * tok, gw), BF16),
            pltpu.VMEM((2 * tok, gw), F32),
            pltpu.VMEM((2, N, gw), F32),
            pltpu.VMEM((2, N, gw), BF16),
            pltpu.VMEM((2, N, gw), BF16),
            pltpu.VMEM((2 * tok, width), BF16),
            pltpu.VMEM((tok, n_x * fw), BF16),
            dma((16,)),
            dma((5,)),
            dma((6,)),
            dma((7,)),
            dma((n_steps,)),
            dma((n_steps,)),
            dma((n_steps, 2)),
            dma((2, heads // G // 2)),
            dma((1,)),
            dma((1,)),
        ],
        compiler_params=pltpu.CompilerParams(
            collective_id=0, has_side_effects=True, vmem_limit_bytes=56 * 1024 * 1024
        ),
    )(
        hidden,
        source_projection,
        gating_projection,
        final_projection,
        entry_mapping_projection,
        readout_mapping_projection,
        increment_projection.T,
        source_conv_taps,
        entry_mapping_taps,
        readout_mapping_taps,
        increment_offsets[None],
        channel_damping_rate[None],
        bypass_coefficients[None],
        stride_multiplier,
        jnp.swapaxes(added_log_damping, 1, 2),
        norm_scale_factor[None],
    )
    return output[None]


def solution(mesh):
    n_grp, n_sp, n_dp = (mesh.shape[a] for a in ("grp", "sp", "dp"))
    return jax.shard_map(
        functools.partial(shards, (n_grp, n_sp, n_dp)),
        mesh=mesh,
        in_specs=(
            P(("grp", "dp"), "sp", None),
            P("dp", None),
            P("dp", None),
            P(),
            P(),
            P(),
            P(),
            P(),
            P(),
            P(),
            P(),
            P(),
            P(("grp", "dp"), None),
            P(("grp", "dp"), None, None),
            P(),
            P(None, "dp"),
        ),
        out_specs=P(("grp", "dp"), "sp", None),
        check_vma=False,
    )
```

time: 46.3 us -> 41.1 us (0.89)
  the two profiles are of different devices: /device:TPU:25 before, /device:TPU:0 now
where the time goes in v1:
time: 41.1 us; the launch traced here: 40.9 us
  Pallas kernels  40 us (97%)
  local copies, waits for them, and re-layouts  0.88 us (2%)
    pallas_call x1, Pallas kernels, shards(): pl.pallas_call(functools.partial(kernel, dims), out_shape=pltpu.VMEM((tok...  40 us
    unnamed x1, local copies, waits for them, and re-layouts  0.88 us

profile of v1, /device:TPU:0, one launch (start us, length us, event | category | flops | bytes accessed | tf_op | source)
XLA Modules:
  0.0 40.9 jit_solution(6377310617279385355)
XLA Ops:
  0.0 40.0 %shard_map.154 = bf16[192,2048]{1,0:T(8,128)(2,1)S(1)} custom-call(bf16[192,2048]{1,0:T(8,128)(2,1)} %bitcast.9, bf16[512,1024]{1,0:T(8,128)(2,1)} %wx_hbm.1, bf16[512,1024]{1,0:T(8,128)(2,1)} %wz_hbm.1, bf16[1024,512]{1,0:T(8,128)(2,1)} %wf_hbm.1, bf16[2048,256]{1,0:T(8,128)(2,1)} %wb_hbm.1, bf16[2048,256]{1,0:T(8,128)(2,1)} %wc_hbm.1, ...), custom_call_target="tpu_custom_call" | custom-call | tf_op jit(solution)/shard_map/pallas_call | solution.py:716
  40.0 0.9 %copy.18 = bf16[1,192,2048]{2,1,0:T(8,128)(2,1)} copy(bf16[1,192,2048]{2,1,0:T(8,128)(2,1)S(1)} %bitcast.8) | data formatting | bytes 1572864

commit v2 on v1

--- a/solution.py
+++ b/solution.py
@@ -17,56 +17,64 @@
 HALO = 16
 CHUNKS = (128, 256, 128)
 TYPES = (2, 2, 4, 4, 3, 4, 3, 4, 2, 4)
-X_ORDER = (("S", 0), ("S", 3), ("S", 1), ("S", 2), ("E", 3), ("S", 4), ("E", 2), ("S", 8), ("S", 5), ("S", 6), ("E", 4), ("S", 7), ("E", 5), ("S", 9), ("E", 6), ("E", 9), ("E", 7))
+X_ORDER = (("S", 3), ("S", 0), ("S", 1), ("S", 2), ("E", 3), ("S", 4), ("S", 8), ("E", 2), ("S", 5), ("S", 7), ("S", 6), ("E", 5), ("S", 9), ("E", 4), ("E", 7), ("E", 6), ("E", 9))
 ORDER = (
+    ("seeds", 3),
     ("seeds", 0),
-    ("seeds", 3),
+    ("seeds", 1),
     "pbc",
-    "nearz",
-    ("relay0", 0),
-    ("relay1", 0),
-    ("seeds", 1),
     ("seeds", 2),
     "nearx",
+    ("relay1", 0),
+    ("relay0", 0),
+    "nearz",
     ("farx", 3),
+    ("relay0", 1),
     ("state", 3),
-    ("relay0", 1),
+    ("relay1", 1),
+    ("seeds", 4),
     ("farx", 0),
-    ("relay1", 1),
     ("state", 0),
-    ("inner", 3),
-    ("seeds", 4),
+    ("seeds", 8),
     ("farx", 2),
     ("state", 2),
     ("farx", 1),
     ("state", 1),
-    ("seeds", 8),
-    ("inner", 1),
     ("relay0", 4),
-    ("inner", 0),
     ("seeds", 5),
     ("relay1", 8),
-    ("farz", 4),
     ("relay0", 8),
+    ("inner", 3),
     ("seeds", 6),
+    ("inner", 0),
     ("seeds", 7),
     ("inner", 2),
+    ("fwd", 8),
     ("farz", 5),
+    ("relay0", 6),
     ("seeds", 9),
-    "finish",
-    ("relay0", 6),
-    "outn",
+    ("farz", 4),
+    ("inner", 1),
+    "finishp",
+    "finisho",
+    ("fwd", 7),
+    ("fwd", 6),
+    "outa",
+    "outb",
+    ("fwd", 9),
     ("out", 8),
-    ("out", 9),
     ("out", 7),
     ("out", 6),
+    ("out", 9),
 )
 SLOTS = (
-    ((0, 30), (1, 30), (2, 28), (3, 29)),
-    ((0, 18), (1, 26), (2, 24), (3, 15)),
-    ((0, 24), (1, 29), (2, 27), (3, 22)),
-    ((0, 30), (1, 34), (2, 34), (3, 33)),
+    ((0, 21), (1, 33), (2, 23), (3, 21)),
+    ((0, 22), (1, 28), (2, 26), (3, 15)),
+    ((0, 23), (1, 28), (2, 27), (3, 20)),
+    ((0, 30), (1, 36), (2, 36), (3, 29)),
 )
+F32 = jnp.float32
+BF16 = jnp.bfloat16
 
 
 def plan(n_sp, n_x, gw, fw):
@@ -80,14 +88,12 @@
     x_order = [(kind, s) for s in every for kind in "SE"]
     order = ["nearz", "pbc", "nearx"]
     for s in every:
-        if steps[s][0] == 2 and "outn" not in order:
-            order += ["finish", "outn"]
         order += [("seeds", s), ("relay0", s)]
-        order += [[("farx", s), ("state", s), ("inner", s)], [("farz", s)], [("out", s)]][steps[s][0]]
-    slots = [[(s, order.index("finish")) for s in every if steps[s][0] == 0]] * 4
+        order += [[("farx", s), ("state", s), ("inner", s)], [("farz", s)], [("fwd", s)]][steps[s][0]]
+    order += ["finishp", "finisho", "outa", "outb"]
+    order += [("out", s) for s in every if steps[s][0] == 2]
+    slots = [[(s, order.index("finishp")) for s in every if steps[s][0] == 0]] * 4
     return steps, [3] * len(steps), x_order, order, slots
-F32 = jnp.float32
-BF16 = jnp.bfloat16
 
 
 def dot(a, b, dims=((1,), (0,)), precision=None):
@@ -147,7 +153,8 @@
     car,
     snd,
     nrm,
-    oth,
+    nsn,
+    acc,
     loc_sem,
     p_send,
     p_recv,
@@ -157,7 +164,7 @@
     relay_recv,
     c_recv,
     n_recv,
-    o_recv,
+    f_recv,
 ):
     n_grp, n_sp, n_dp = dims
     n_x = n_dp // 2
@@ -170,8 +177,8 @@
     rows_dev = wx_hbm.shape[0]
     fw = wf_hbm.shape[1]
     width = wf_hbm.shape[0]
-    halo_send, x_send, y_send, z_send, c_send, n_send, o_send = (link_send.at[i] for i in range(7))
-    halo_recv = p_recv.at[5]
+    halo_send, x_send, y_send, z_send, c_send, n_send, f_send = (link_send.at[i] for i in range(7))
+    halo_recv = p_recv.at[6]
     own_cols = pl.ds(pl.multiple_of(core * gw, 128), gw)
     other_cols = pl.ds(pl.multiple_of((1 - core) * gw, 128), gw)
     partner = {"dp": xi * 2 + 1 - core}
@@ -220,8 +227,8 @@
         locals_.append(copy)
         return copy
 
-    def far_rows(chip):
-        return pl.ds(pl.multiple_of(chip * width, 128), width)
+    def out_rows(d):
+        return pl.ds(pl.multiple_of(d * width, 128), width)
 
     def seq_rows(s):
         return pl.ds(s * tok, tok)
@@ -240,7 +247,7 @@
     maps += [local(wc_hbm.at[:, group_n], wbc.at[:, pl.ds(N, N)])]
     maps += [local(tb_hbm.at[:, group_n], tb), local(tc_hbm.at[:, group_n], tc)]
     own = [local(srcs[w].at[:, own_cols], bufs[w].at[dev_rows]) for w in range(2)]
-    own += [local(wf_hbm, wf.at[far_rows(xi)])]
+    own += [local(wf_hbm, wf.at[out_rows(dp)])]
     late = [local(tx_hbm.at[:, own_cols], tx), local(skip_hbm, skip), local(scale_hbm.at[:, own_cols], scale)]
 
     greeted = 2 + 2 * (n_x - 1) + 2 * jnp.minimum(z, 1) + 2 * jnp.minimum(n_sp - 1 - z, 1)
@@ -260,7 +267,7 @@
     def place(s, chip, q, k):
         w, j, cw = steps[s]
         size = piece_rows(s)
-        row = chip * width + (q * 2 + k) * size if w == 2 else (chip * 2 + k) * rows_dev + q * size
+        row = (chip * 2 + core) * width + (q * 2 + k) * size if w == 2 else (chip * 2 + k) * rows_dev + q * size
         return bufs[w].at[pl.ds(pl.multiple_of(row, 16), size), pl.ds(j * cw, cw)]
 
     def origin(s, q, k, d):
@@ -354,6 +361,7 @@
             start(remote(damp_hbm.at[0, other_heads], damp.at[core], p_send.at[2], p_recv.at[2], partner))
             for w in range(2):
                 start(remote(srcs[w].at[:, other_cols], bufs[w].at[dev_rows], p_send.at[3 + w], p_recv.at[3 + w], partner))
+            start(remote(wf_hbm, wf.at[out_rows(dp)], p_send.at[5], p_recv.at[5], partner))
 
     def seeds(s):
         pieces_wait(s, 2, seed_recv.at[s])
@@ -559,52 +567,75 @@
     def step_cols(s):
         return pl.ds(steps[s][1] * steps[s][2], steps[s][2])
 
-    def slot_rows(s, swap):
-        return pl.ds(pl.multiple_of(lax.rem(s + core + swap, 2) * tok, 16), tok)
-
-    def finish(s):
-        reached = dot(cm[seq_rows(s), :], car[s])
+    dp_pair = (dp, xi * 2 + 1 - core)
+
+    def seq_rows_of(mine):
+        return pl.ds(pl.multiple_of((core if mine else 1 - core) * tok, 16), tok)
+
+    def finish(mine):
+        seq = core if mine else 1 - core
+        rows = seq_rows_of(mine)
+        reached = dot(cm[rows, :], car[seq])
+        reach_s = jnp.where(seq == 0, reach[:, 0:per_group], reach[:, per_group : 2 * per_group])
         square = jnp.zeros((tok, 1), F32)
         for p in range(pairs):
             pc = pair_cols(p)
             here = slice(p * 2 * P_SIZE, (p + 1) * 2 * P_SIZE)
-            mixed = y[seq_rows(s), pc] + spread(reach, s * pairs + p, first_head) * reached[:, here]
-            gated = mixed.astype(BF16).astype(F32) * gz[seq_rows(s), pc]
+            mixed = y[rows, pc] + spread(reach_s, p, first_head) * reached[:, here]
+            gated = mixed.astype(BF16).astype(F32) * gz[rows, pc]
             square = square + jnp.sum(gated * gated, axis=1, keepdims=True)
-            y[seq_rows(s), pc] = gated
+            y[rows, pc] = gated
         inv = lax.rsqrt(square * (1.0 / gw) + EPSILON)
-        nrm[slot_rows(s, 0), own_cols] = (y[seq_rows(s), :] * inv * scale[...]).astype(BF16)
-        remote(
-            nrm.at[slot_rows(s, 0), own_cols], nrm.at[slot_rows(s, 1), own_cols],
-            n_send, n_recv.at[0], partner,
-        ).start()
-
-    def out_cols(o, s, d):
+        normed = (y[rows, :] * inv * scale[...]).astype(BF16)
+        if mine:
+            nrm[:, own_cols] = normed
+        else:
+            nsn[...] = normed
+            remote(nsn, nrm.at[:, own_cols], n_send, n_recv.at[0], partner).start()
+
+    def half_k(d, cols, group_cols):
+        first = pl.multiple_of(d * width + group_cols.start, 128)
+        return dot(nrm[:, group_cols], wf[pl.ds(first, gw), cols])
+
+    def out_a():
+        own[2].wait()
+        spot = wf.at[out_rows(dp_pair[1])]
+        remote(spot, spot, p_send.at[5], p_recv.at[5], partner).wait_recv()
+        for i, d in enumerate(dp_pair):
+            for j in range(0, fw, tile):
+                cols = pl.ds(j, tile)
+                acc[i, :, cols] = half_k(d, cols, own_cols)
+
+    def out_b():
+        spot = nrm.at[:, other_cols]
+        remote(nsn, spot, n_send, n_recv.at[0], partner).wait_recv()
+        for i, d in enumerate(dp_pair):
+            for j in range(0, fw, tile):
+                cols = pl.ds(j, tile)
+                whole_cols = pl.ds(pl.multiple_of(d * fw + j, 128), tile)
+                out_ref[:, whole_cols] = (acc[i, :, cols] + half_k(d, cols, other_cols)).astype(BF16)
+
+    def forward_copy(o, s):
+        spot = wf.at[out_rows(owner_of(o) * 2 + core), step_cols(s)]
+        return remote(spot, spot, f_send, f_recv.at[f_steps.index(s)], partner)
+
+    def forward(s):
+        rest(s)
+        for o in range(1, n_x):
+            forward_copy(o, s).start()
+
+    def output(s):
         cols = step_cols(s)
-        return pl.ds(pl.multiple_of((owner_of(o) * 2 + d) * fw + cols.start, 128), cols.size)
-
-    def out_copy(o, s, d):
-        cols = step_cols(s)
-        return remote(
-            oth.at[:, pl.ds(o * fw + cols.start, cols.size)], out_ref.at[:, out_cols(o, s, d)],
-            o_send, o_recv.at[0], partner,
-        )
-
-    def output(o, s):
-        cols = step_cols(s)
-        part = dot(nrm[...], wf[far_rows(owner_of(o)), cols]).astype(BF16)
-        out_ref[:, out_cols(o, s, core)] = part[0:tok, :]
-        oth[:, pl.ds(o * fw + cols.start, cols.size)] = part[tok : 2 * tok, :]
-        out_copy(o, s, core).start()
+        spot = wf.at[pl.ds(0, (n_x - 1) * width), cols]
+        remote(spot, spot, f_send, f_recv.at[f_steps.index(s)], partner).wait_recv()
+        for o in range(1, n_x):
+            for d in (core, 1 - core):
+                owner = owner_of(o) * 2 + d
+                whole_cols = pl.ds(pl.multiple_of(owner * fw + cols.start, 128), cols.size)
+                out_ref[:, whole_cols] = dot(nrm[...], wf[out_rows(owner), cols]).astype(BF16)
 
     f_steps = [s for s in range(len(steps)) if steps[s][0] == 2]
-
-    def out_near():
-        own[2].wait()
-        spot = nrm.at[:, other_cols]
-        remote(spot, spot, n_send, n_recv.at[0], partner).wait_recv()
-        for s in f_steps:
-            output(0, s)
+    tile = min(256, fw)
 
     def run(name):
         if name == "nearz":
@@ -615,11 +646,14 @@
         elif name == "nearx":
             near(0)
             tiles(gw, 256, near_x)
-        elif name == "finish":
-            for s in range(2):
-                finish(s)
-        elif name == "outn":
-            out_near()
+        elif name == "finishp":
+            finish(False)
+        elif name == "finisho":
+            finish(True)
+        elif name == "outa":
+            out_a()
+        elif name == "outb":
+            out_b()
         else:
             task, s = name
             cols = step_cols(s)
@@ -638,10 +672,10 @@
             elif task == "farz":
                 rest(s)
                 far_z(cols)
+            elif task == "fwd":
+                forward(s)
             else:
-                rest(s)
-                for o in range(1, n_x):
-                    output(o, s)
+                output(s)
 
     for n, name in enumerate(order):
         for level in (1, 2, 3):
@@ -649,7 +683,6 @@
                 if at == n:
                     chain_slot(level, step_cols(s))
         run(name)
-    remote(oth, oth, o_send, o_recv.at[0], partner).wait_recv()
 
     def sent_wait(send, rows):
         if rows:
@@ -669,9 +702,9 @@
             def _(k=k):
                 sent_wait(x_send, sent["x"][k])
 
-    spot = nrm.at[:, own_cols]
-    remote(spot, spot, n_send, n_recv.at[0], partner).wait_send()
-    remote(oth, oth, o_send, o_recv.at[0], partner).wait_send()
+    remote(nsn, nsn, n_send, n_recv.at[0], partner).wait_send()
+    spot = wf.at[pl.ds(0, (n_x - 1) * width)]
+    remote(spot, spot, f_send, n_recv.at[0], partner).wait_send()
 
     @pl.when(z < n_sp - 1)
     def _():
@@ -709,7 +742,9 @@
     fw = final_projection.shape[1]
     length = stride_multiplier.shape[1]
     out_width = fw * n_dp
-    n_steps = len(plan(n_sp, n_x, gw, fw)[0])
+    steps = plan(n_sp, n_x, gw, fw)[0]
+    n_steps = len(steps)
+    n_far = sum(1 for step in steps if step[0] == 2)
     span = HALO + tok
     dma = pltpu.SemaphoreType.DMA
     hbm = pl.BlockSpec(memory_space=pl.ANY)
@@ -722,7 +757,7 @@
             pltpu.VMEM((2 * span, model), BF16),
             pltpu.VMEM((model, gw), BF16),
             pltpu.VMEM((model, gw), BF16),
-            pltpu.VMEM((n_x * width, fw), BF16),
+            pltpu.VMEM((n_dp * width, fw), BF16),
             pltpu.VMEM((model, 2 * N), BF16),
             pltpu.VMEM((heads, model), BF16),
             pltpu.VMEM((CONV_W, gw), F32),
@@ -748,18 +783,19 @@
             pltpu.VMEM((2, N, gw), F32),
             pltpu.VMEM((2, N, gw), BF16),
             pltpu.VMEM((2, N, gw), BF16),
-            pltpu.VMEM((2 * tok, width), BF16),
-            pltpu.VMEM((tok, n_x * fw), BF16),
+            pltpu.VMEM((tok, width), BF16),
+            pltpu.VMEM((tok, gw), BF16),
+            pltpu.VMEM((2, tok, fw), F32),
             dma((16,)),
-            dma((5,)),
             dma((6,)),
+            dma((7,)),
             dma((7,)),
             dma((n_steps,)),
             dma((n_steps,)),
             dma((n_steps, 2)),
             dma((2, heads // G // 2)),
             dma((1,)),
-            dma((1,)),
+            dma((n_far,)),
         ],
         compiler_params=pltpu.CompilerParams(
             collective_id=0, has_side_effects=True, vmem_limit_bytes=56 * 1024 * 1024

time: 41.1 us -> 37.8 us (0.920)
  Pallas kernels: 40 us -> 36.7 us
    pallas_call x1, Pallas kernels: 40 us -> 36.7 us  [shards(): pl.pallas_call(functools.partial(kernel, dims), out_shape=pltpu.VMEM((tok...]
where the time goes in v2:
time: 37.8 us; the launch traced here: 37.6 us
  Pallas kernels  36.7 us (97%)
  local copies, waits for them, and re-layouts  0.88 us (2%)
    pallas_call x1, Pallas kernels, shards(): pl.pallas_call(functools.partial(kernel, dims), out_shape=pltpu.VMEM((tok...  36.7 us
    unnamed x1, local copies, waits for them, and re-layouts  0.88 us

profile of v2, /device:TPU:0, one launch (start us, length us, event | category | flops | bytes accessed | tf_op | source)
XLA Modules:
  0.0 37.6 jit_solution(11914670832857726351)
XLA Ops:
  0.0 36.7 %shard_map.154 = bf16[192,2048]{1,0:T(8,128)(2,1)S(1)} custom-call(bf16[192,2048]{1,0:T(8,128)(2,1)} %bitcast.9, bf16[512,1024]{1,0:T(8,128)(2,1)} %wx_hbm.1, bf16[512,1024]{1,0:T(8,128)(2,1)} %wz_hbm.1, bf16[1024,512]{1,0:T(8,128)(2,1)} %wf_hbm.1, bf16[2048,256]{1,0:T(8,128)(2,1)} %wb_hbm.1, bf16[2048,256]{1,0:T(8,128)(2,1)} %wc_hbm.1, ...), custom_call_target="tpu_custom_call" | custom-call | tf_op jit(solution)/shard_map/pallas_call | solution.py:751
  36.7 0.9 %copy.18 = bf16[1,192,2048]{2,1,0:T(8,128)(2,1)} copy(bf16[1,192,2048]{2,1,0:T(8,128)(2,1)S(1)} %bitcast.8) | data formatting | bytes 1572864

commit v3 on v2

--- a/solution.py
+++ b/solution.py
@@ -16,62 +16,62 @@
 MESH = pl.DeviceIdType.MESH
 HALO = 16
 CHUNKS = (128, 256, 128)
-TYPES = (2, 2, 4, 4, 3, 4, 3, 4, 2, 4)
-X_ORDER = (("S", 3), ("S", 0), ("S", 1), ("S", 2), ("E", 3), ("S", 4), ("S", 8), ("E", 2), ("S", 5), ("S", 7), ("S", 6), ("E", 5), ("S", 9), ("E", 4), ("E", 7), ("E", 6), ("E", 9))
+TYPES = (4, 2, 2, 4, 4, 3, 3, 4, 4, 2)
+X_ORDER = (("S", 3), ("S", 1), ("S", 2), ("S", 0), ("E", 3), ("S", 5), ("S", 9), ("E", 0), ("S", 6), ("S", 4), ("S", 7), ("S", 8), ("E", 5), ("E", 4), ("E", 8), ("E", 6), ("E", 7))
 ORDER = (
     ("seeds", 3),
+    ("seeds", 1),
+    ("seeds", 2),
+    "pbc",
+    ("relay0", 1),
     ("seeds", 0),
-    ("seeds", 1),
-    "pbc",
-    ("seeds", 2),
     "nearx",
-    ("relay1", 0),
-    ("relay0", 0),
-    "nearz",
     ("farx", 3),
-    ("relay0", 1),
+    ("relay1", 1),
     ("state", 3),
-    ("relay1", 1),
-    ("seeds", 4),
-    ("farx", 0),
-    ("state", 0),
-    ("seeds", 8),
+    ("relay1", 2),
+    ("relay0", 2),
+    ("seeds", 5),
+    ("seeds", 9),
+    ("farx", 1),
     ("farx", 2),
     ("state", 2),
-    ("farx", 1),
+    ("inner", 3),
+    ("farx", 0),
+    ("relay0", 5),
     ("state", 1),
-    ("relay0", 4),
-    ("seeds", 5),
-    ("relay1", 8),
-    ("relay0", 8),
-    ("inner", 3),
+    ("state", 0),
     ("seeds", 6),
+    ("seeds", 4),
+    ("relay1", 9),
+    "nearz",
+    ("relay0", 9),
     ("inner", 0),
+    ("seeds", 8),
+    ("inner", 2),
+    ("inner", 1),
+    ("relay0", 6),
+    ("farz", 5),
     ("seeds", 7),
-    ("inner", 2),
+    ("farz", 4),
+    ("gate", 1),
     ("fwd", 8),
-    ("farz", 5),
-    ("relay0", 6),
-    ("seeds", 9),
-    ("farz", 4),
-    ("inner", 1),
+    ("fwd", 9),
+    ("gate", 0),
     "finishp",
     "finisho",
+    ("fwd", 6),
     ("fwd", 7),
-    ("fwd", 6),
     "outa",
     "outb",
-    ("fwd", 9),
-    ("out", 8),
-    ("out", 7),
-    ("out", 6),
-    ("out", 9),
+    ("out", 1),
+    ("out", 0),
 )
 SLOTS = (
-    ((0, 21), (1, 33), (2, 23), (3, 21)),
-    ((0, 22), (1, 28), (2, 26), (3, 15)),
-    ((0, 23), (1, 28), (2, 27), (3, 20)),
-    ((0, 30), (1, 36), (2, 36), (3, 29)),
+    ((0, 24), (1, 33), (2, 30), (3, 27)),
+    ((0, 29), (1, 26), (2, 23), (3, 13)),
+    ((0, 33), (1, 30), (2, 28), (3, 19)),
+    ((0, 38), (1, 37), (2, 35), (3, 24)),
 )
 F32 = jnp.float32
 BF16 = jnp.bfloat16
@@ -90,9 +90,10 @@
     for s in every:
         order += [("seeds", s), ("relay0", s)]
         order += [[("farx", s), ("state", s), ("inner", s)], [("farz", s)], [("fwd", s)]][steps[s][0]]
+    order += [("gate", j) for j in range(gw // 256)]
     order += ["finishp", "finisho", "outa", "outb"]
-    order += [("out", s) for s in every if steps[s][0] == 2]
-    slots = [[(s, order.index("finishp")) for s in every if steps[s][0] == 0]] * 4
+    order += [("out", j) for j in range(max(fw // 256, 1))]
+    slots = [[(s, order.index(("gate", 0))) for s in every if steps[s][0] == 0]] * 4
     return steps, [3] * len(steps), x_order, order, slots
 
 
@@ -261,6 +262,11 @@
         direct.append({2: (), 3: (turn,), 4: (0, 1)}[kind])
         relayed.append(tuple(k for k in (0, 1) if k not in direct[-1]))
 
+    relay_slots = [(s, k) for s in range(len(steps)) for k in relayed[s]]
+
+    def relay_sem(s, k):
+        return relay_recv.at[relay_slots.index((s, k))]
+
     def piece_rows(s):
         return width // 8 if steps[s][0] == 2 else rows_dev // 4
 
@@ -327,7 +333,7 @@
 
     def z_start(s, o, k):
         spot = place(s, owner_of(o), own_q, k)
-        recv = relay_recv.at[s, k] if k in relayed[s] else rest_recv.at[s]
+        recv = relay_sem(s, k) if k in relayed[s] else rest_recv.at[s]
         remote(spot, spot, z_send, recv, z_peer).start()
         sent["z"] += unit(s)
 
@@ -373,7 +379,7 @@
 
     def relay(s, r):
         k = relayed[s][r]
-        pieces_wait(s, 1, relay_recv.at[s, k])
+        pieces_wait(s, 1, relay_sem(s, k))
         for o in range(1, n_x):
             y_start(s, o, z_q, k)
 
@@ -572,21 +578,21 @@
     def seq_rows_of(mine):
         return pl.ds(pl.multiple_of((core if mine else 1 - core) * tok, 16), tok)
 
+    def gate(j):
+        cols = pl.ds(j * block, block)
+        for s in range(2):
+            reached = dot(cm[seq_rows(s), :], car[s, :, cols])
+            for p in step_pairs(cols):
+                pc = pair_cols(p)
+                here = slice(p * 2 * P_SIZE - cols.start, (p + 1) * 2 * P_SIZE - cols.start)
+                mixed = y[seq_rows(s), pc] + spread(reach, s * pairs + p, first_head) * reached[:, here]
+                y[seq_rows(s), pc] = mixed.astype(BF16).astype(F32) * gz[seq_rows(s), pc]
+
     def finish(mine):
-        seq = core if mine else 1 - core
-        rows = seq_rows_of(mine)
-        reached = dot(cm[rows, :], car[seq])
-        reach_s = jnp.where(seq == 0, reach[:, 0:per_group], reach[:, per_group : 2 * per_group])
-        square = jnp.zeros((tok, 1), F32)
-        for p in range(pairs):
-            pc = pair_cols(p)
-            here = slice(p * 2 * P_SIZE, (p + 1) * 2 * P_SIZE)
-            mixed = y[rows, pc] + spread(reach_s, p, first_head) * reached[:, here]
-            gated = mixed.astype(BF16).astype(F32) * gz[rows, pc]
-            square = square + jnp.sum(gated * gated, axis=1, keepdims=True)
-            y[rows, pc] = gated
+        gated = y[seq_rows_of(mine), :]
+        square = jnp.sum(gated * gated, axis=1, keepdims=True)
         inv = lax.rsqrt(square * (1.0 / gw) + EPSILON)
-        normed = (y[rows, :] * inv * scale[...]).astype(BF16)
+        normed = (gated * inv * scale[...]).astype(BF16)
         if mine:
             nrm[:, own_cols] = normed
         else:
@@ -624,10 +630,12 @@
         for o in range(1, n_x):
             forward_copy(o, s).start()
 
-    def output(s):
-        cols = step_cols(s)
-        spot = wf.at[pl.ds(0, (n_x - 1) * width), cols]
-        remote(spot, spot, f_send, f_recv.at[f_steps.index(s)], partner).wait_recv()
+    def output(j):
+        cols = pl.ds(j * tile, tile)
+        for s in f_steps:
+            if step_cols(s).start // tile == j:
+                spot = wf.at[pl.ds(0, (n_x - 1) * width), step_cols(s)]
+                remote(spot, spot, f_send, f_recv.at[f_steps.index(s)], partner).wait_recv()
         for o in range(1, n_x):
             for d in (core, 1 - core):
                 owner = owner_of(o) * 2 + d
@@ -636,6 +644,7 @@
 
     f_steps = [s for s in range(len(steps)) if steps[s][0] == 2]
     tile = min(256, fw)
+    block = 256
 
     def run(name):
         if name == "nearz":
@@ -656,22 +665,23 @@
             out_b()
         else:
             task, s = name
-            cols = step_cols(s)
             if task == "seeds":
                 seeds(s)
             elif task in ("relay0", "relay1"):
                 relay(s, int(task[-1]))
             elif task == "farx":
                 rest(s)
-                far_x(cols)
+                far_x(step_cols(s))
             elif task == "state":
-                local_state(cols)
+                local_state(step_cols(s))
             elif task == "inner":
                 for q in range(2):
-                    inner(q, cols)
+                    inner(q, step_cols(s))
             elif task == "farz":
                 rest(s)
-                far_z(cols)
+                far_z(step_cols(s))
+            elif task == "gate":
+                gate(s)
             elif task == "fwd":
                 forward(s)
             else:
@@ -742,7 +752,8 @@
     fw = final_projection.shape[1]
     length = stride_multiplier.shape[1]
     out_width = fw * n_dp
-    steps = plan(n_sp, n_x, gw, fw)[0]
+    steps, types = plan(n_sp, n_x, gw, fw)[:2]
+    n_relay = sum(4 - kind for kind in types)
     n_steps = len(steps)
     n_far = sum(1 for step in steps if step[0] == 2)
     span = HALO + tok
@@ -792,7 +803,7 @@
             dma((7,)),
             dma((n_steps,)),
             dma((n_steps,)),
-            dma((n_steps, 2)),
+            dma((max(n_relay, 1),)),
             dma((2, heads // G // 2)),
             dma((1,)),
             dma((n_far,)),

time: 37.8 us -> 37 us (0.979)
  Pallas kernels: 36.7 us -> 35.9 us
    pallas_call x1, Pallas kernels: 36.7 us -> 35.9 us  [shards(): pl.pallas_call(functools.partial(kernel, dims), out_shape=pltpu.VMEM((tok...]
where the time goes in v3:
time: 37 us; the launch traced here: 36.8 us
  Pallas kernels  35.9 us (97%)
  local copies, waits for them, and re-layouts  0.88 us (2%)
    pallas_call x1, Pallas kernels, shards(): pl.pallas_call(functools.partial(kernel, dims), out_shape=pltpu.VMEM((tok...  35.9 us
    unnamed x1, local copies, waits for them, and re-layouts  0.88 us

profile of v3, /device:TPU:0, one launch (start us, length us, event | category | flops | bytes accessed | tf_op | source)
XLA Modules:
  0.0 36.8 jit_solution(16025064422426405587)
XLA Ops:
  0.0 35.9 %shard_map.154 = bf16[192,2048]{1,0:T(8,128)(2,1)S(1)} custom-call(bf16[192,2048]{1,0:T(8,128)(2,1)} %bitcast.9, bf16[512,1024]{1,0:T(8,128)(2,1)} %wx_hbm.1, bf16[512,1024]{1,0:T(8,128)(2,1)} %wz_hbm.1, bf16[1024,512]{1,0:T(8,128)(2,1)} %wf_hbm.1, bf16[2048,256]{1,0:T(8,128)(2,1)} %wb_hbm.1, bf16[2048,256]{1,0:T(8,128)(2,1)} %wc_hbm.1, ...), custom_call_target="tpu_custom_call" | custom-call | tf_op jit(solution)/shard_map/pallas_call | solution.py:762
  35.9 0.9 %copy.18 = bf16[1,192,2048]{2,1,0:T(8,128)(2,1)} copy(bf16[1,192,2048]{2,1,0:T(8,128)(2,1)S(1)} %bitcast.8) | data formatting | bytes 1572864

commit v4 on v3

--- a/solution.py
+++ b/solution.py
@@ -16,51 +16,52 @@
 MESH = pl.DeviceIdType.MESH
 HALO = 16
 CHUNKS = (128, 256, 128)
-TYPES = (4, 2, 2, 4, 4, 3, 3, 4, 4, 2)
-X_ORDER = (("S", 3), ("S", 1), ("S", 2), ("S", 0), ("E", 3), ("S", 5), ("S", 9), ("E", 0), ("S", 6), ("S", 4), ("S", 7), ("S", 8), ("E", 5), ("E", 4), ("E", 8), ("E", 6), ("E", 7))
+TYPES = (4, 2, 4, 2, 4, 2, 4, 4, 4, 4)
+ACROSS = (0, 0, 0, 0, 0, 0, 1, 0, 1, 0)
+X_ORDER = (("S", 1), ("S", 3), ("S", 2), ("E", 2), ("S", 0), ("S", 5), ("E", 0), ("S", 8), ("S", 6), ("S", 4), ("S", 9), ("E", 8), ("E", 6), ("S", 7), ("E", 4), ("E", 9), ("E", 7))
 ORDER = (
+    ("seeds", 1),
     ("seeds", 3),
-    ("seeds", 1),
     ("seeds", 2),
+    ("relay0", 1),
     "pbc",
-    ("relay0", 1),
+    "nearx",
+    ("relay0", 3),
+    ("relay1", 3),
     ("seeds", 0),
-    "nearx",
-    ("farx", 3),
+    "nearz",
     ("relay1", 1),
-    ("state", 3),
-    ("relay1", 2),
-    ("relay0", 2),
-    ("seeds", 5),
-    ("seeds", 9),
-    ("farx", 1),
     ("farx", 2),
     ("state", 2),
+    ("seeds", 5),
+    ("farx", 3),
+    ("state", 3),
+    ("farx", 0),
+    ("state", 0),
+    ("seeds", 8),
+    ("farx", 1),
+    ("state", 1),
+    ("seeds", 6),
+    ("relay1", 5),
+    ("relay0", 5),
+    ("seeds", 4),
+    ("inner", 2),
+    ("cross", 6),
+    ("cross", 8),
+    ("inner", 0),
     ("inner", 3),
-    ("farx", 0),
-    ("relay0", 5),
-    ("state", 1),
-    ("state", 0),
-    ("seeds", 6),
-    ("seeds", 4),
-    ("relay1", 9),
-    "nearz",
-    ("relay0", 9),
-    ("inner", 0),
-    ("seeds", 8),
-    ("inner", 2),
+    ("seeds", 9),
+    ("seeds", 7),
+    ("farz", 5),
+    ("farz", 4),
     ("inner", 1),
-    ("relay0", 6),
-    ("farz", 5),
-    ("seeds", 7),
-    ("farz", 4),
+    ("fwd", 6),
     ("gate", 1),
     ("fwd", 8),
-    ("fwd", 9),
     ("gate", 0),
     "finishp",
+    ("fwd", 9),
     "finisho",
-    ("fwd", 6),
     ("fwd", 7),
     "outa",
     "outb",
@@ -68,10 +69,10 @@
     ("out", 0),
 )
 SLOTS = (
-    ((0, 24), (1, 33), (2, 30), (3, 27)),
-    ((0, 29), (1, 26), (2, 23), (3, 13)),
-    ((0, 33), (1, 30), (2, 28), (3, 19)),
-    ((0, 38), (1, 37), (2, 35), (3, 24)),
+    ((0, 22), (1, 28), (2, 26), (3, 20)),
+    ((0, 26), (1, 30), (2, 16), (3, 22)),
+    ((0, 29), (1, 31), (2, 22), (3, 28)),
+    ((0, 36), (1, 38), (2, 32), (3, 32)),
 )
 F32 = jnp.float32
 BF16 = jnp.bfloat16
@@ -83,7 +84,7 @@
         cw = min(CHUNKS[w], wide)
         steps += [(w, j, cw) for j in range(wide // cw)]
     if (n_sp, n_x, len(steps)) == (4, 2, len(TYPES)):
-        return steps, TYPES, X_ORDER, ORDER, SLOTS
+        return steps, TYPES, ACROSS, X_ORDER, ORDER, SLOTS
     every = range(len(steps))
     x_order = [(kind, s) for s in every for kind in "SE"]
     order = ["nearz", "pbc", "nearx"]
@@ -94,7 +95,7 @@
     order += ["finishp", "finisho", "outa", "outb"]
     order += [("out", j) for j in range(max(fw // 256, 1))]
     slots = [[(s, order.index(("gate", 0))) for s in every if steps[s][0] == 0]] * 4
-    return steps, [3] * len(steps), x_order, order, slots
+    return steps, [3] * len(steps), [0] * len(steps), x_order, order, slots
 
 
 def dot(a, b, dims=((1,), (0,)), precision=None):
@@ -254,7 +255,7 @@
     greeted = 2 + 2 * (n_x - 1) + 2 * jnp.minimum(z, 1) + 2 * jnp.minimum(n_sp - 1 - z, 1)
     pl.semaphore_wait(barrier, greeted)
 
-    steps, types, x_order, order, slots = plan(n_sp, n_x, gw, fw)
+    steps, types, across, x_order, order, slots = plan(n_sp, n_x, gw, fw)
     last_step = len(steps) - 1
     direct, relayed = [], []
     for kind in types:
@@ -263,6 +264,7 @@
         relayed.append(tuple(k for k in (0, 1) if k not in direct[-1]))
 
     relay_slots = [(s, k) for s in range(len(steps)) for k in relayed[s]]
+    relay_slots += [(s, "across") for s in range(len(steps)) if across[s]]
 
     def relay_sem(s, k):
         return relay_recv.at[relay_slots.index((s, k))]
@@ -285,7 +287,8 @@
     def owner_of(o):
         return lax.rem(xi - o + n_x, n_x)
 
-    sent = {"x": [0, 0], "y": 0, "z": 0}
+    sent = {(c, b): 0 for c in range(2) for b in range(2)}
+    sent.update(y=0, z=0, across=0)
 
     def x_start(s, o, q, k, d, recv):
         peer = {"dp": lax.rem(xi + o, n_x) * 2 + d}
@@ -302,33 +305,36 @@
             else:
                 for d in (core, 1 - core):
                     x_start(s, o, own_q, core, d, seed_recv)
-            for k in range(2):
-                sent["x"][k] += 2 * unit(s)
+            for key in ((0, 0), (0, 1), (1, 0), (1, 1)):
+                sent[key] += 2 * unit(s)
 
     def x_extras(s):
         for o in range(1, n_x):
-            if steps[s][0] == 2:
-                for k in direct[s]:
-                    x_start(s, o, far_q, k, core, rest_recv)
-                    sent["x"][0] += unit(s)
-                    sent["x"][1] += unit(s)
-            elif len(direct[s]) == 2:
-                for d in (core, 1 - core):
-                    x_start(s, o, far_q, core, d, rest_recv)
-                sent["x"][0] += 2 * unit(s)
-                sent["x"][1] += 2 * unit(s)
-            else:
-                for k in direct[s]:
-                    sent["x"][k] += 2 * unit(s)
-
-                    @pl.when(core == k)
-                    def _(k=k, o=o):
-                        for d in (core, 1 - core):
-                            x_start(s, o, far_q, k, d, rest_recv)
-
-    def y_start(s, o, q, k):
+            for n, k in enumerate(direct[s]):
+                odd_only = bool(across[s]) and n == 0
+                near_only = steps[s][0] != 2
+                sides = (1,) if odd_only else (0, 1)
+                for c in (k,) if near_only else (0, 1):
+                    for b in sides:
+                        sent[c, b] += (2 if near_only else 1) * unit(s)
+
+                def go(k=k, o=o):
+                    for d in (core, 1 - core) if near_only else (core,):
+                        x_start(s, o, far_q, k, d, rest_recv)
+
+                if near_only and odd_only:
+                    pl.when(jnp.logical_and(core == k, zb == 1))(go)
+                elif near_only:
+                    pl.when(core == k)(go)
+                elif odd_only:
+                    pl.when(zb == 1)(go)
+                else:
+                    go()
+
+    def y_start(s, o, q, k, turned=False):
         spot = place(s, owner_of(o), q, k)
-        remote(spot, spot, y_send, rest_recv.at[s], y_peer).start()
+        recv = relay_sem(s, "across") if turned else rest_recv.at[s]
+        remote(spot, spot, y_send, recv, y_peer).start()
         sent["y"] += unit(s)
 
     def z_start(s, o, k):
@@ -374,8 +380,19 @@
         for o in range(1, n_x):
             for k in relayed[s] + direct[s]:
                 z_start(s, o, k)
-            for k in range(2):
-                y_start(s, o, own_q, k)
+            for k in direct[s] + relayed[s]:
+                y_start(s, o, own_q, k, bool(across[s]) and k == direct[s][0])
+
+    def cross(s):
+        k = direct[s][0]
+        pieces_wait(s, 1, relay_sem(s, "across"))
+        sent["across"] += (n_x - 1) * unit(s)
+
+        @pl.when(zb == 1)
+        def _():
+            for o in range(1, n_x):
+                spot = place(s, owner_of(o), y_q, k)
+                remote(spot, spot, z_send, rest_recv.at[s], z_peer).start()
 
     def relay(s, r):
         k = relayed[s][r]
@@ -384,7 +401,7 @@
             y_start(s, o, z_q, k)
 
     def rest(s):
-        pieces_wait(s, 6 - len(relayed[s]), rest_recv.at[s])
+        pieces_wait(s, 6 - len(relayed[s]) - across[s], rest_recv.at[s])
 
     depth = 2 * rows_dev
 
@@ -667,6 +684,8 @@
             task, s = name
             if task == "seeds":
                 seeds(s)
+            elif task == "cross":
+                cross(s)
             elif task in ("relay0", "relay1"):
                 relay(s, int(task[-1]))
             elif task == "farx":
@@ -702,15 +721,19 @@
     for copy in sends:
         copy.wait_send()
     sent_wait(y_send, sent["y"])
-    sent_wait(z_send, sent["z"])
-    if sent["x"][0] == sent["x"][1]:
-        sent_wait(x_send, sent["x"][0])
-    else:
-        for k in range(2):
-
-            @pl.when(core == k)
-            def _(k=k):
-                sent_wait(x_send, sent["x"][k])
+    for b in range(2):
+
+        @pl.when(zb == b)
+        def _(b=b):
+            sent_wait(z_send, sent["z"] + b * sent["across"])
+            if sent[0, b] == sent[1, b]:
+                sent_wait(x_send, sent[0, b])
+            else:
+                for c in range(2):
+
+                    @pl.when(core == c)
+                    def _(c=c):
+                        sent_wait(x_send, sent[c, b])
 
     remote(nsn, nsn, n_send, n_recv.at[0], partner).wait_send()
     spot = wf.at[pl.ds(0, (n_x - 1) * width)]
@@ -752,8 +775,8 @@
     fw = final_projection.shape[1]
     length = stride_multiplier.shape[1]
     out_width = fw * n_dp
-    steps, types = plan(n_sp, n_x, gw, fw)[:2]
-    n_relay = sum(4 - kind for kind in types)
+    steps, types, across = plan(n_sp, n_x, gw, fw)[:3]
+    n_relay = sum(4 - kind for kind in types) + sum(across)
     n_steps = len(steps)
     n_far = sum(1 for step in steps if step[0] == 2)
     span = HALO + tok

time: 37 us -> 36.3 us (0.981)
  Pallas kernels: 35.9 us -> 35.2 us
    pallas_call x1, Pallas kernels: 35.9 us -> 35.2 us  [shards(): pl.pallas_call(functools.partial(kernel, dims), out_shape=pltpu.VMEM((tok...]
where the time goes in v4:
time: 36.3 us; the launch traced here: 36.1 us
  Pallas kernels  35.2 us (97%)
  local copies, waits for them, and re-layouts  0.88 us (2%)
    pallas_call x1, Pallas kernels, shards(): pl.pallas_call(functools.partial(kernel, dims), out_shape=pltpu.VMEM((tok...  35.2 us
    unnamed x1, local copies, waits for them, and re-layouts  0.88 us

profile of v4, /device:TPU:0, one launch (start us, length us, event | category | flops | bytes accessed | tf_op | source)
XLA Modules:
  0.0 36.1 jit_solution(11828125718819485946)
XLA Ops:
  0.0 35.2 %shard_map.154 = bf16[192,2048]{1,0:T(8,128)(2,1)S(1)} custom-call(bf16[192,2048]{1,0:T(8,128)(2,1)} %bitcast.9, bf16[512,1024]{1,0:T(8,128)(2,1)} %wx_hbm.1, bf16[512,1024]{1,0:T(8,128)(2,1)} %wz_hbm.1, bf16[1024,512]{1,0:T(8,128)(2,1)} %wf_hbm.1, bf16[2048,256]{1,0:T(8,128)(2,1)} %wb_hbm.1, bf16[2048,256]{1,0:T(8,128)(2,1)} %wc_hbm.1, ...), custom_call_target="tpu_custom_call" | custom-call | tf_op jit(solution)/shard_map/pallas_call | solution.py:785
  35.3 0.9 %copy.18 = bf16[1,192,2048]{2,1,0:T(8,128)(2,1)} copy(bf16[1,192,2048]{2,1,0:T(8,128)(2,1)S(1)} %bitcast.8) | data formatting | bytes 1572864

commit v5 on v4

--- a/solution.py
+++ b/solution.py
@@ -51,8 +51,8 @@
     ("inner", 0),
     ("inner", 3),
     ("seeds", 9),
+    ("farz", 5),
     ("seeds", 7),
-    ("farz", 5),
     ("farz", 4),
     ("inner", 1),
     ("fwd", 6),
@@ -372,8 +372,8 @@
             start(remote(stride_hbm, stride.at[core], p_send.at[1], p_recv.at[1], partner))
             start(remote(damp_hbm.at[0, other_heads], damp.at[core], p_send.at[2], p_recv.at[2], partner))
             for w in range(2):
-                start(remote(srcs[w].at[:, other_cols], bufs[w].at[dev_rows], p_send.at[3 + w], p_recv.at[3 + w], partner))
-            start(remote(wf_hbm, wf.at[out_rows(dp)], p_send.at[5], p_recv.at[5], partner))
+                remote(srcs[w].at[:, other_cols], bufs[w].at[dev_rows], p_send.at[3], p_recv.at[3 + w], partner).start()
+            remote(wf_hbm, wf.at[out_rows(dp)], p_send.at[3], p_recv.at[5], partner).start()
 
     def seeds(s):
         pieces_wait(s, 2, seed_recv.at[s])
@@ -465,7 +465,7 @@
     def near(w):
         own[w].wait()
         spot = bufs[w].at[partner_rows]
-        remote(spot, spot, p_send.at[3 + w], p_recv.at[3 + w], partner).wait_recv()
+        remote(spot, spot, p_send.at[3], p_recv.at[3 + w], partner).wait_recv()
 
     def tiles(width, tile, body):
         def run(j, carry):
@@ -623,7 +623,7 @@
     def out_a():
         own[2].wait()
         spot = wf.at[out_rows(dp_pair[1])]
-        remote(spot, spot, p_send.at[5], p_recv.at[5], partner).wait_recv()
+        remote(spot, spot, p_send.at[3], p_recv.at[5], partner).wait_recv()
         for i, d in enumerate(dp_pair):
             for j in range(0, fw, tile):
                 cols = pl.ds(j, tile)
@@ -720,6 +720,7 @@
 
     for copy in sends:
         copy.wait_send()
+    sent_wait(p_send.at[3], 2 * rows_dev + width * fw // gw)
     sent_wait(y_send, sent["y"])
     for b in range(2):
 
@@ -821,7 +822,7 @@
             pltpu.VMEM((tok, gw), BF16),
             pltpu.VMEM((2, tok, fw), F32),
             dma((16,)),
-            dma((6,)),
+            dma((4,)),
             dma((7,)),
             dma((7,)),
             dma((n_steps,)),

time: 36.3 us -> 36.3 us (level)
  no operation moved by 1% of the time
where the time goes in v5:
time: 36.3 us; the launch traced here: 36.1 us
  Pallas kernels  35.2 us (97%)
  local copies, waits for them, and re-layouts  0.88 us (2%)
    pallas_call x1, Pallas kernels, shards(): pl.pallas_call(functools.partial(kernel, dims), out_shape=pltpu.VMEM((tok...  35.2 us
    unnamed x1, local copies, waits for them, and re-layouts  0.88 us

profile of v5, /device:TPU:0, one launch (start us, length us, event | category | flops | bytes accessed | tf_op | source)
XLA Modules:
  0.0 36.1 jit_solution(13599885604718684083)
XLA Ops:
  0.0 35.2 %shard_map.154 = bf16[192,2048]{1,0:T(8,128)(2,1)S(1)} custom-call(bf16[192,2048]{1,0:T(8,128)(2,1)} %bitcast.9, bf16[512,1024]{1,0:T(8,128)(2,1)} %wx_hbm.1, bf16[512,1024]{1,0:T(8,128)(2,1)} %wz_hbm.1, bf16[1024,512]{1,0:T(8,128)(2,1)} %wf_hbm.1, bf16[2048,256]{1,0:T(8,128)(2,1)} %wb_hbm.1, bf16[2048,256]{1,0:T(8,128)(2,1)} %wc_hbm.1, ...), custom_call_target="tpu_custom_call" | custom-call | tf_op jit(solution)/shard_map/pallas_call | solution.py:786
  35.2 0.9 %copy.18 = bf16[1,192,2048]{2,1,0:T(8,128)(2,1)} copy(bf16[1,192,2048]{2,1,0:T(8,128)(2,1)S(1)} %bitcast.8) | data formatting | bytes 1572864
